TPU v7x, 32 devices: a whole 2x2x4 slice. The times are simulated.
32 devices in a mesh: sp: 16 (over z, y, x), tp: 2 (over core).
Axes of the slice: x: 2, y: 2, z: 4, core: 2. Of those that a mesh axis runs over, the one named last changes fastest.
Arguments:
- tokens: bfloat16 [1024, 1, 2048], P('sp'), may hold values from -6 to 6
- queries: bfloat16 [1024, 1, 1024], P('sp', None, 'tp'), may hold values from -15 to 15
- key_values: bfloat16 [1024, 1, 1024], P('sp', None, 'tp'), may hold values from -6 to 6
- stop_bias: bfloat16 [1024, 1, 16], P('sp', None, 'tp'), may hold values from -20 to 0
- out_proj: bfloat16 [1024, 2048], P('tp'), may hold values from -0.375 to 0.375
- norm_gain: float32 [2048], replicated, may hold values from 0.1 to 1.9
- up_proj: bfloat16 [2048, 4096], P('sp', 'tp'), may hold values from -0.125 to 0.125
- down_proj: bfloat16 [4096, 2048], P('tp', 'sp'), may hold values from -0.09375 to 0.09375
Outputs:
- layer_out: bfloat16 [1024, 1, 2048], P(('sp', 'tp'))
All inputs are finite; a program needn't handle non-finite values.
Results may differ from a plain program's by a relative error of at most 0.018.
Values may be sent and summed in bfloat16 or wider, within the bound.
A program may use at most 64 MiB of HBM per device.

v0:
```python
import math

import jax
import jax.numpy as jnp
from jax import lax
from jax.experimental import pallas as pl
from jax.experimental.pallas import tpu as pltpu
from jax.sharding import PartitionSpec as P

HEAD = 64


EPSILON = 1e-06


def rms_scale(residual, gain):
    values = residual.astype(jnp.float32)
    factor = lax.rsqrt(jnp.mean(values * values, axis=-1, keepdims=True) + EPSILON)
    return (values * factor * gain).astype(jnp.bfloat16)


def sweep_keys(totals, pieces, shard_rows, step_fn):
    kv_rows, bias_rows = pieces
    shards = kv_rows.shape[0] // shard_rows
    group_shards = math.gcd(shards, max(1, 1024 // shard_rows))
    span_rows = group_shards * shard_rows

    def advance(number, running):
        first_row = number * span_rows
        kv_block = lax.dynamic_slice_in_dim(kv_rows, first_row, span_rows, 0)
        bias_block = lax.dynamic_slice_in_dim(bias_rows, first_row, span_rows, 0)
        return step_fn(running, kv_block, bias_block, first_row, group_shards)

    return lax.fori_loop(0, shards // group_shards, advance, totals)


def general_body(tokens, queries, key_values, stop_bias, out_proj, norm_gain, up_proj, down_proj):
    row_count = tokens.shape[0]
    seq_count = tokens.shape[1]
    head_count = queries.shape[2] // HEAD
    kv_count = key_values.shape[2] // (2 * HEAD)
    group_size = head_count // kv_count
    n_shards = lax.axis_size("sp")
    query_start = lax.axis_index("sp") * row_count
    query_pos = query_start + lax.iota(jnp.int32, row_count)
    q_heads = queries.reshape(row_count, seq_count, kv_count, group_size, HEAD).transpose(
        1, 2, 3, 0, 4
    )
    q_heads = q_heads.reshape(seq_count, kv_count, group_size * row_count, HEAD)

    def stick_block(kv_block, bias_block, key_start):
        span_rows = kv_block.shape[0]
        key_pairs = kv_block.reshape(span_rows, seq_count, kv_count, 2 * HEAD)
        keys_part = key_pairs[..., :HEAD]
        values_part = key_pairs[..., HEAD:]
        scores = (
            jnp.einsum("bgmd,sbgd->bgms", q_heads, keys_part, preferred_element_type=jnp.float32)
            * 0.125
        )
        bias_float = jnp.transpose(bias_block, (1, 2, 0)).astype(jnp.float32)
        scores = (
            scores.reshape(seq_count, head_count, row_count, span_rows) + bias_float[:, :, None, :]
        )
        key_pos = key_start + lax.iota(jnp.int32, span_rows)
        strict = key_pos[None, :] < query_pos[:, None]
        log_pass = jnp.where(strict, jax.nn.log_sigmoid(-scores), 0.0)
        return (scores, strict, log_pass, values_part)

    def weigh(scores, strict, after_sum, values_part):
        span_rows = scores.shape[3]
        weights = jnp.where(strict, jnp.exp(jax.nn.log_sigmoid(scores) + after_sum), 0.0).astype(
            jnp.bfloat16
        )
        weights = weights.reshape(seq_count, kv_count, group_size * row_count, span_rows)
        return jnp.einsum(
            "bgms,sbgd->bgmd", weights, values_part, preferred_element_type=jnp.float32
        )

    empty_out = jnp.zeros((seq_count, kv_count, group_size * row_count, HEAD), jnp.float32)

    def sum_step(sums_table, kv_block, bias_block, key_start, shard_group):

        def sum_compute(table_in):
            scores, strict, log_pass, values_part = stick_block(kv_block, bias_block, key_start)
            block_sums = log_pass.reshape(
                seq_count, head_count, row_count, shard_group, row_count
            ).sum(axis=4)
            slot_index = key_start // row_count
            current = lax.dynamic_slice_in_dim(table_in, slot_index, shard_group, 0)
            return lax.dynamic_update_slice_in_dim(
                table_in, current + jnp.transpose(block_sums, (3, 0, 1, 2)), slot_index, 0
            )

        return lax.cond(
            key_start < query_start + row_count, sum_compute, lambda table_in: table_in, sums_table
        )

    empty_table = jnp.zeros((n_shards, seq_count, head_count, row_count), jnp.float32)
    sums_table = sweep_keys(
        empty_table,
        (
            lax.all_gather(key_values, "sp", axis=0, tiled=True),
            lax.all_gather(stop_bias, "sp", axis=0, tiled=True),
        ),
        row_count,
        sum_step,
    )
    offsets = lax.cumsum(sums_table, axis=0, reverse=True) - sums_table

    def out_step(outputs, kv_block, bias_block, key_start, shard_group):

        def out_compute(running):
            scores, strict, log_pass, values_part = stick_block(kv_block, bias_block, key_start)
            span_rows = kv_block.shape[0]
            split_pass = log_pass.reshape(seq_count, head_count, row_count, shard_group, row_count)
            within = lax.cumsum(split_pass, axis=4, reverse=True) - split_pass
            carried = lax.dynamic_slice_in_dim(offsets, key_start // row_count, shard_group, 0)
            carried = jnp.transpose(carried, (1, 2, 3, 0))[..., None]
            after_sum = (within + carried).reshape(seq_count, head_count, row_count, span_rows)
            return running + weigh(scores, strict, after_sum, values_part)

        return lax.cond(
            key_start < query_start + row_count, out_compute, lambda running: running, outputs
        )

    accum_out = sweep_keys(
        empty_out,
        (
            lax.all_gather(key_values, "sp", axis=0, tiled=True),
            lax.all_gather(stop_bias, "sp", axis=0, tiled=True),
        ),
        row_count,
        out_step,
    )
    attended = accum_out.reshape(seq_count, kv_count, group_size, row_count, HEAD).transpose(
        3, 0, 1, 2, 4
    )
    attended = attended.reshape(row_count * seq_count, head_count * HEAD).astype(jnp.bfloat16)
    share_tokens = row_count // lax.axis_size("tp")
    share_rows = share_tokens * seq_count
    tp_index = lax.axis_index("tp")
    projected = lax.psum(
        jnp.dot(attended, out_proj, preferred_element_type=jnp.float32).astype(jnp.bfloat16), "tp"
    ).astype(jnp.float32)
    flat_tokens = tokens.reshape(row_count * seq_count, tokens.shape[2])
    residual = (flat_tokens.astype(jnp.float32) + projected).astype(jnp.bfloat16)
    normed = rms_scale(residual, norm_gain)
    residual_share = lax.dynamic_slice_in_dim(residual, tp_index * share_rows, share_rows, 0)
    up_values = jnp.dot(
        normed,
        lax.all_gather(up_proj, "sp", axis=0, tiled=True),
        preferred_element_type=jnp.float32,
    )
    hidden = jnp.square(jax.nn.relu(up_values)).astype(jnp.bfloat16)
    partial_terms = jnp.dot(
        hidden,
        lax.all_gather(down_proj, "sp", axis=1, tiled=True),
        preferred_element_type=jnp.float32,
    )
    update = lax.psum_scatter(
        partial_terms.astype(jnp.bfloat16), "tp", scatter_dimension=0, tiled=True
    ).astype(jnp.float32)
    result = (residual_share.astype(jnp.float32) + update).astype(jnp.bfloat16)
    return result.reshape(share_tokens, seq_count, result.shape[1])


MESH = pl.DeviceIdType.MESH
LO = 4
LANES = 128
F32 = jnp.float32
BF16 = jnp.bfloat16


def remote(src, dst, send, recv, sp, tp):
    return pltpu.make_async_remote_copy(
        src_ref=src,
        dst_ref=dst,
        send_sem=send,
        recv_sem=recv,
        device_id={"sp": sp, "tp": tp},
        device_id_type=MESH,
    )


def dot_nt(a, b):
    return lax.dot_general(a, b, (((1,), (1,)), ((), ())), preferred_element_type=F32)


def dot_tn(a, b):
    return lax.dot_general(a, b, (((0,), (0,)), ((), ())), preferred_element_type=F32)


def layer_kernel(
    HI,
    G,
    tok_ref,
    q_ref,
    kvp_ref,
    bias_ref,
    wo_hbm,
    gain_ref,
    up_ref,
    dn_ref,
    out_ref,
    kvb_ref,
    wo_ref,
    load_sem,
    kv_buf,
    up_buf,
    dn_buf,
    q_buf,
    tri_buf,
    carry,
    acc,
    att_buf,
    pj_buf,
    pj_in,
    res_buf,
    n_buf,
    hid_buf,
    ps_buf,
    x_in,
    xs_buf,
    pr_buf,
    kv_sz,
    kv_sp,
    kv_recv,
    kv_half,
    wz_send,
    up_sp,
    up_recv,
    up_half,
    dn_sp,
    dn_recv,
    dn_half,
    pj_send,
    pj_recv,
    n_send,
    nf_send,
    n_recv,
    x_send,
    x_recv,
    p_send,
    p_recv,
):
    s = lax.axis_index("sp")
    c = lax.axis_index("tp")
    hi = s // LO
    lo = s % LO
    lo1 = lo + 1 - 2 * (lo % 2)
    lo2 = (lo + 2) % LO
    lo3 = (lo1 + 2) % LO
    other = 1 - c
    T = q_ref.shape[0]
    H = T // 2
    D = tok_ref.shape[1]
    R = up_ref.shape[0]
    CH = up_buf.shape[1]
    W = dn_ref.shape[1]
    KW = G * LANES
    PL = LO * T
    own_cols = pl.ds(pl.multiple_of(hi * CH, LANES), CH)

    barrier = pltpu.get_barrier_semaphore()
    for p in (lo1, lo2):
        pl.semaphore_signal(barrier, inc=1, device_id={"sp": hi * LO + p, "tp": c}, device_id_type=MESH)
    pl.semaphore_signal(barrier, inc=1, device_id={"sp": s, "tp": other}, device_id_type=MESH)
    for dz in range(1, HI):
        far = ((hi + dz) % HI) * LO + lo
        pl.semaphore_signal(barrier, inc=1, device_id={"sp": far, "tp": c}, device_id_type=MESH)
    loads = [
        pltpu.make_async_copy(wo_hbm, wo_ref, load_sem.at[0]),
        pltpu.make_async_copy(up_ref.at[:, own_cols], up_buf.at[pl.ds(s * R, R)], load_sem.at[1]),
        pltpu.make_async_copy(dn_ref.at[pl.ds(hi * CH, CH)], dn_buf.at[s], load_sem.at[2]),
    ]
    for load in loads:
        load.start()
    kvb_ref[:, :KW] = kvp_ref[...]
    kvb_ref[:, KW:] = jnp.zeros((T, LANES), BF16)
    kvb_ref[:, KW : KW + 2 * G] = bias_ref[...]
    pl.semaphore_wait(barrier, 3 + (HI - 1))

    class Piece:
        def __init__(self, view, rows, send, recv, half):
            self.view, self.rows, self.send, self.recv, self.half = view, rows, send, recv, half

        def full(self, j):
            return self.view(j, 0, self.rows)

        def part(self, j, h):
            return self.view(j, h * (self.rows // 2), self.rows // 2)

        def direct(self, z, src=None):
            j = z * LO + lo
            src = self.full(j) if src is None else src
            return [
                remote(src, self.full(j), self.send.at[z * 4 + k], self.recv.at[j], hi * LO + p, c)
                for k, p in enumerate((lo1, lo2))
            ]

        def diag(self, z):
            a, b = z * LO + lo1, z * LO + lo2
            first, last = self.part(a, 0), self.part(b, 1)
            return [
                remote(first, first, self.send.at[z * 4 + 2], self.recv.at[a], hi * LO + lo2, c),
                remote(last, last, self.send.at[z * 4 + 3], self.half.at[z], hi * LO + lo1, c),
            ]

        def arrived(self, ref, sem):
            remote(ref, ref, self.send.at[0], sem, s, other).wait_recv()

        def wait_own(self, z):
            j = z * LO + lo
            self.arrived(self.full(j), self.recv.at[j])

        def wait_direct(self, z):
            for p in (lo1, lo2):
                j = z * LO + p
                self.arrived(self.full(j), self.recv.at[j])

        def wait_diag(self, z):
            j = z * LO + lo3
            self.arrived(self.part(j, 0), self.recv.at[j])
            self.arrived(self.part(j, 1), self.half.at[z])

    kv = Piece(lambda j, r, n: kv_buf.at[pl.ds(j * T + r, n)], T, kv_sp, kv_recv, kv_half)
    up = Piece(lambda j, r, n: up_buf.at[pl.ds(j * R + r, n)], R, up_sp, up_recv, up_half)
    dn = Piece(lambda j, r, n: dn_buf.at[j, pl.ds(r, n)], CH, dn_sp, dn_recv, dn_half)
    up_own = up_ref.at[:, own_cols]
    dn_own = dn_ref.at[pl.ds(hi * CH, CH)]

    def start(copies):
        for copy in copies:
            copy.start()

    def below(dz):
        return (hi - dz + HI) % HI

    def kv_up(hp):
        return remote(kvb_ref, kv.full(s), kv_sz.at[hp], kv_recv.at[s], hp * LO + lo, c)

    def up_far(hp):
        cols = pl.ds(hp * CH, CH)
        return remote(up_ref.at[:, cols], up.full(s), wz_send.at[2 * hp], up_recv.at[s], hp * LO + lo, c)

    def dn_far(hp):
        rows = pl.ds(hp * CH, CH)
        return remote(dn_ref.at[rows], dn.full(s), wz_send.at[2 * hp + 1], dn_recv.at[s], hp * LO + lo, c)

    for hp in range(HI):

        @pl.when(hp > hi)
        def _():
            kv_up(hp).start()

    start(kv.direct(hi, kvb_ref))
    for far in (up_far, dn_far):
        for hp in range(HI - 2, -1, -1):

            @pl.when(hp < hi)
            def _():
                far(hp).start()

    start(up.direct(hi, up_own))
    kv_buf[pl.ds(s * T, T), :] = kvb_ref[...]
    lane = lax.broadcasted_iota(jnp.int32, (T, LANES), 1)
    low = lane < HEAD
    for g in range(G):
        qg = q_ref[:, g * LANES : (g + 1) * LANES].astype(F32) * 0.125
        first = jnp.where(low, qg, 0.0)
        second = jnp.where(low, pltpu.roll(qg, HEAD, 1), 0.0)
        q_buf[g] = jnp.concatenate([first, second], axis=0).astype(BF16)
    row_id = lax.broadcasted_iota(jnp.int32, (PL, PL), 0)
    col_id = lax.broadcasted_iota(jnp.int32, (PL, PL), 1)
    tri_buf[...] = jnp.where(col_id > row_id, 1.0, 0.0).astype(BF16)
    carry[...] = jnp.zeros_like(carry)
    acc[...] = jnp.zeros_like(acc)

    sel_row = lax.broadcasted_iota(jnp.int32, (LANES, LANES), 0) // HEAD
    sel_lane = lax.broadcasted_iota(jnp.int32, (LANES, LANES), 1)
    key_row = lax.broadcasted_iota(jnp.int32, (PL, LANES), 0)
    query_pos = s * T + lax.broadcasted_iota(jnp.int32, (PL, LANES), 1) % T

    def attend(plane):
        rows = pl.ds(plane * PL, PL)
        bias = kv_buf[rows, KW : KW + LANES]
        strict = plane * PL + key_row < query_pos
        for g in range(G):
            pairs = kv_buf[rows, g * LANES : (g + 1) * LANES]
            pick = jnp.where(sel_lane == 2 * g + sel_row, 1.0, 0.0).astype(BF16)
            scores = dot_nt(pairs, q_buf[g]) + dot_nt(bias, pick)
            soft = jnp.maximum(scores, 0.0) + jnp.log(1.0 + jnp.exp(-jnp.abs(scores)))
            log_pass = jnp.where(strict, -soft, 0.0)
            top = log_pass.astype(BF16)
            rest = (log_pass - top.astype(F32)).astype(BF16)
            after = jnp.dot(tri_buf[...], top, preferred_element_type=F32) + jnp.dot(
                tri_buf[...], rest, preferred_element_type=F32
            )
            held = carry[g]
            weights = jnp.where(strict, jnp.exp(scores - soft + after + held), 0.0).astype(BF16)
            acc[g] += dot_tn(weights, pairs)
            carry[g] = held + after[0:1] + log_pass[0:1]

    def column(k):
        @pl.when(k <= hi)
        def _():
            kv.wait_own(hi - k)
            start(kv.direct(hi - k))

    def relay(k):
        @pl.when(k <= hi)
        def _():
            kv.wait_direct(hi - k)
            start(kv.diag(hi - k))

    def look(k):
        @pl.when(k <= hi)
        def _():
            kv.wait_diag(hi - k)
            attend(hi - k)

    def up_column(dz):
        up.wait_own(below(dz))
        start(up.direct(below(dz)))

    def up_relay(dz):
        up.wait_direct(below(dz))
        start(up.diag(below(dz)))

    def dn_column(dz):
        dn.wait_own(below(dz))
        start(dn.direct(below(dz)))

    def dn_relay(dz):
        dn.wait_direct(below(dz))
        start(dn.diag(below(dz)))

    for k in range(1, HI):
        column(k)
        relay(k - 1)
        if k == 1:
            for far in (up_far, dn_far):
                for hp in range(1, HI):

                    @pl.when(hp > hi)
                    def _():
                        far(hp).start()

        if k >= 2:
            look(k - 2)
    relay(HI - 1)
    up_column(1)
    up_relay(0)
    if HI >= 2:
        look(HI - 2)
    for dz in range(2, HI):
        up_column(dz)
    start(dn.direct(hi, dn_own))
    look(HI - 1)
    up_relay(1)

    for load in loads:
        load.wait()
    for g in range(G):
        a0 = pltpu.roll(acc[g, 0:T, :], HEAD, 1)
        a1 = acc[g, T : 2 * T, :]
        att_buf[:, g * LANES : (g + 1) * LANES] = jnp.where(low, a0, a1).astype(BF16)
    att = att_buf[...]
    wide = 512 if D % 512 == 0 else LANES
    for i in range(D // wide):
        cols = slice(i * wide, (i + 1) * wide)
        pj_buf[:, cols] = jnp.dot(att, wo_ref[:, cols], preferred_element_type=F32).astype(BF16)

    pj_copy = remote(pj_buf.at[pl.ds(other * H, H)], pj_in, pj_send, pj_recv, s, other)
    pj_copy.start()
    for dz in range(2, HI):
        up_relay(dz)
    pj_copy.wait()
    mine = pl.ds(c * H, H)
    total = pj_buf[mine, :].astype(F32) + pj_in[...].astype(F32)
    residual = (tok_ref[mine, :].astype(F32) + total).astype(BF16)
    res_buf[...] = residual
    values = residual.astype(F32)
    factor = lax.rsqrt(jnp.mean(values * values, axis=-1, keepdims=True) + EPSILON)

    def n_at(z, core):
        return n_buf.at[pl.ds((core * HI + z) * H, H)]

    n_buf[pl.ds((c * HI + hi) * H, H), :] = (values * factor * gain_ref[...]).astype(BF16)

    def n_out(dz):
        hp = (hi + dz) % HI
        return remote(n_at(hi, c), n_at(hi, c), n_send.at[dz], n_recv.at[c * HI + hi], hp * LO + lo, c)

    def n_pass(dz):
        z = below(dz)
        return remote(n_at(z, c), n_at(z, c), nf_send.at[dz], n_recv.at[c * HI + z], s, other)

    def n_wait(z, core):
        ref = n_at(z, core)
        remote(ref, ref, nf_send.at[0], n_recv.at[core * HI + z], s, other).wait_recv()

    for dz in range(1, HI):
        n_out(dz).start()
    n_pass(0).start()
    for dz in range(1, HI):
        dn_column(dz)
    dn_relay(0)
    for dz in range(1, HI):
        n_wait(below(dz), c)
        n_pass(dz).start()
    for dz in range(HI):
        up.wait_diag(below(dz))
    for dz in range(HI):
        n_wait(below(dz), other)

    step = 256 if CH % 256 == 0 else LANES
    for i in range(CH // step):
        cols = slice(i * step, (i + 1) * step)
        raw = jnp.maximum(jnp.dot(n_buf[...], up_buf[:, cols], preferred_element_type=F32), 0.0)
        hid_buf[:, cols] = (raw * raw).astype(BF16)

    half = HI * H

    def x_out(dz):
        z = below(dz)
        rows = pl.ds(other * half, half)
        return remote(ps_buf.at[z, rows], x_in.at[z], x_send.at[dz], x_recv.at[z], s, other)

    def p_out(dz, far):
        z = below(dz)
        hp = (hi + far) % HI
        return remote(
            xs_buf.at[z, pl.ds(hp * H, H)],
            pr_buf.at[hi, z],
            p_send.at[dz * HI + far],
            p_recv.at[hi * HI + z],
            hp * LO + lo,
            c,
        )

    def p_wait(src, z):
        ref = pr_buf.at[src, z]
        remote(ref, ref, p_send.at[0], p_recv.at[src * HI + z], s, other).wait_recv()

    def spread(dz):
        z = below(dz)
        x_in_ref = x_in.at[z]
        remote(x_in_ref, x_in_ref, x_send.at[0], x_recv.at[z], s, other).wait_recv()
        mixed = ps_buf[z, pl.ds(c * half, half), :].astype(F32) + x_in[z].astype(F32)
        xs_buf[z] = mixed.astype(BF16)
        for far in range(1, HI):
            p_out(dz, far).start()

    for dz in range(HI):
        if dz + 1 < HI:
            dn_relay(dz + 1)
        z = below(dz)
        dn.wait_diag(z)
        for q in range(0, LO, 2):
            pair = jnp.concatenate([dn_buf[z * LO + q], dn_buf[z * LO + q + 1]], axis=1)
            part = jnp.dot(hid_buf[...], pair, preferred_element_type=F32)
            ps_buf[z, :, q * W : (q + 2) * W] = part.astype(BF16)
        x_out(dz).start()
        if dz > 0:
            spread(dz - 1)
    spread(HI - 1)
    CW = LO * W
    for dz in range(HI):
        z = below(dz)
        cols = pl.ds(pl.multiple_of(z * CW, LANES), CW)
        update = xs_buf[z, pl.ds(hi * H, H), :].astype(F32)
        for far in range(1, HI):
            p_wait(below(far), z)
            update = update + pr_buf[below(far), z].astype(F32)
        out_ref[:, cols] = (res_buf[:, cols].astype(F32) + update).astype(BF16)

    for hp in range(HI):

        @pl.when(hp > hi)
        def _():
            kv_up(hp).wait_send()

        @pl.when(hp <= hi)
        def _():
            for copy in kv.direct(hp) + kv.diag(hp):
                copy.wait_send()

        @pl.when(hp != hi)
        def _():
            up_far(hp).wait_send()
            dn_far(hp).wait_send()

        for copy in up.direct(hp) + up.diag(hp) + dn.direct(hp) + dn.diag(hp):
            copy.wait_send()

    for dz in range(HI):
        n_pass(dz).wait_send()
        x_out(dz).wait_send()
        if dz > 0:
            n_out(dz).wait_send()
        for far in range(1, HI):
            p_out(dz, far).wait_send()


def fits(tokens, queries, key_values, stop_bias, up_proj, down_proj):
    sp = lax.axis_size("sp")
    rows, seqs, heads = stop_bias.shape
    hidden = up_proj.shape[1]
    return (
        lax.axis_size("tp") == 2
        and sp % LO == 0
        and sp > LO
        and seqs == 1
        and heads <= LANES
        and queries.shape[2] == heads * HEAD
        and key_values.shape[2] == heads * HEAD
        and 2 * HEAD == LANES
        and 2 * rows == LANES
        and hidden % (sp // LO * LANES) == 0
        and down_proj.shape[1] % LANES == 0
        and up_proj.shape[0] % 16 == 0
        and tokens.shape[2] % LANES == 0
    )


def body(tokens, queries, key_values, stop_bias, out_proj, norm_gain, up_proj, down_proj):
    if not fits(tokens, queries, key_values, stop_bias, up_proj, down_proj):
        return general_body(
            tokens, queries, key_values, stop_bias, out_proj, norm_gain, up_proj, down_proj
        )
    sp = lax.axis_size("sp")
    HI = sp // LO
    T, _, D = tokens.shape
    H = T // 2
    heads = stop_bias.shape[2]
    G = heads // 2
    R, hidden = up_proj.shape
    CH = hidden // HI
    W = down_proj.shape[1]
    KB = G * LANES + LANES
    vmem = pl.BlockSpec(memory_space=pltpu.VMEM)
    hbm = pl.BlockSpec(memory_space=pl.ANY)
    dma = pltpu.SemaphoreType.DMA
    out = pl.pallas_call(
        lambda *refs: layer_kernel(HI, G, *refs),
        out_shape=jax.ShapeDtypeStruct((H, D), BF16),
        in_specs=[vmem, vmem, vmem, vmem, hbm, vmem, hbm, hbm],
        out_specs=vmem,
        scratch_shapes=[
            pltpu.VMEM((T, KB), BF16),
            pltpu.VMEM(out_proj.shape, BF16),
            dma((3,)),
            pltpu.VMEM((sp * T, KB), BF16),
            pltpu.VMEM((sp * R, CH), BF16),
            pltpu.VMEM((sp, CH, W), BF16),
            pltpu.VMEM((G, LANES, LANES), BF16),
            pltpu.VMEM((LO * T, LO * T), BF16),
            pltpu.VMEM((G, 1, LANES), F32),
            pltpu.VMEM((G, LANES, LANES), F32),
            pltpu.VMEM((T, G * LANES), BF16),
            pltpu.VMEM((T, D), BF16),
            pltpu.VMEM((H, D), BF16),
            pltpu.VMEM((H, D), BF16),
            pltpu.VMEM((HI * T, D), BF16),
            pltpu.VMEM((HI * T, CH), BF16),
            pltpu.VMEM((HI, HI * T, LO * W), BF16),
            pltpu.VMEM((HI, HI * H, LO * W), BF16),
            pltpu.VMEM((HI, HI * H, LO * W), BF16),
            pltpu.VMEM((HI, HI, H, LO * W), BF16),
            dma((HI,)),
            dma((HI * 4,)),
            dma((sp,)),
            dma((HI,)),
            dma((HI * 2,)),
            dma((HI * 4,)),
            dma((sp,)),
            dma((HI,)),
            dma((HI * 4,)),
            dma((sp,)),
            dma((HI,)),
            dma,
            dma,
            dma((HI,)),
            dma((HI,)),
            dma((HI * 2,)),
            dma((HI,)),
            dma((HI,)),
            dma((HI * HI,)),
            dma((HI * HI,)),
        ],
        compiler_params=pltpu.CompilerParams(
            collective_id=0, has_side_effects=True, vmem_limit_bytes=56 * 1024 * 1024
        ),
        name="layer",
    )(
        tokens.reshape(T, D),
        queries.reshape(T, queries.shape[2]),
        key_values.reshape(T, key_values.shape[2]),
        stop_bias.reshape(T, heads),
        out_proj,
        norm_gain.reshape(1, D),
        up_proj,
        down_proj,
    )
    return out.reshape(H, 1, D)


def solution(mesh):
    return jax.shard_map(
        body,
        mesh=mesh,
        in_specs=(
            P("sp", None, None),
            P("sp", None, "tp"),
            P("sp", None, "tp"),
            P("sp", None, "tp"),
            P("tp", None),
            P(),
            P("sp", "tp"),
            P("tp", "sp"),
        ),
        out_specs=P(("sp", "tp"), None, None),
        check_vma=False,
    )
```

profile of v0, /device:TPU:0, one launch (start us, length us, event | category | flops | bytes accessed | tf_op | source)
XLA Modules:
  0.0 74.1 jit_solution(169558143279739895)
XLA Ops:
  0.0 1.4 %copy.9 = bf16[64,1,8]{2,0,1:T(8,128)(2,1)} copy(bf16[64,1,8]{0,2,1:T(8,128)(2,1)} %param.11) | data formatting | bytes 2048 | tf_op args[3]
  1.4 71.1 %layer.1 = bf16[32,2048]{1,0:T(8,128)(2,1)} custom-call(bf16[64,2048]{1,0:T(8,128)(2,1)} %bitcast.7, bf16[64,512]{1,0:T(8,128)(2,1)} %bitcast.8, bf16[64,512]{1,0:T(8,128)(2,1)} %bitcast.9, bf16[64,8]{1,0:T(8,128)(2,1)} %bitcast.10, bf16[512,2048]{1,0:T(8,128)(2,1)} %refs_4_.1, f32[1,2048]{1,0:T(1,128)} %bitcast.11, bf16[128,2048]{1,0:T(8,128)(2,1)} %refs_6_.1, ...), custom_call_target="tpu_custom_call" | custom-call | tf_op jit(solution)/shard_map/layer/pallas_call | solution.py:645
  72.5 1.6 %copy.11 = bf16[32,1,2048]{2,0,1:T(8,128)(2,1)} copy(bf16[32,1,2048]{2,0,1:T(8,128)(2,1)} %bitcast.6) | data formatting | bytes 262144
where the time goes:
time: 74.3 us; the launch traced here: 74.1 us
  Pallas kernels  71.1 us (96%)
  local copies, waits for them, and re-layouts  2.94 us (4%)
    pallas_call x1, Pallas kernels, body(): pl.pallas_call(lambda *refs: layer_kernel(HI, G, *refs), out_shape=jax.Sh...  71.1 us
    unnamed x2, local copies, waits for them, and re-layouts  2.94 us

commit v1 on v0

v1 whole, which is shorter than its diff:
```python
import math

import jax
import jax.numpy as jnp
from jax import lax
from jax.experimental import pallas as pl
from jax.experimental.pallas import tpu as pltpu
from jax.sharding import PartitionSpec as P

HEAD = 64


EPSILON = 1e-06


def rms_scale(residual, gain):
    values = residual.astype(jnp.float32)
    factor = lax.rsqrt(jnp.mean(values * values, axis=-1, keepdims=True) + EPSILON)
    return (values * factor * gain).astype(jnp.bfloat16)


def sweep_keys(totals, pieces, shard_rows, step_fn):
    kv_rows, bias_rows = pieces
    shards = kv_rows.shape[0] // shard_rows
    group_shards = math.gcd(shards, max(1, 1024 // shard_rows))
    span_rows = group_shards * shard_rows

    def advance(number, running):
        first_row = number * span_rows
        kv_block = lax.dynamic_slice_in_dim(kv_rows, first_row, span_rows, 0)
        bias_block = lax.dynamic_slice_in_dim(bias_rows, first_row, span_rows, 0)
        return step_fn(running, kv_block, bias_block, first_row, group_shards)

    return lax.fori_loop(0, shards // group_shards, advance, totals)


def general_body(tokens, queries, key_values, stop_bias, out_proj, norm_gain, up_proj, down_proj):
    row_count = tokens.shape[0]
    seq_count = tokens.shape[1]
    head_count = queries.shape[2] // HEAD
    kv_count = key_values.shape[2] // (2 * HEAD)
    group_size = head_count // kv_count
    n_shards = lax.axis_size("sp")
    query_start = lax.axis_index("sp") * row_count
    query_pos = query_start + lax.iota(jnp.int32, row_count)
    q_heads = queries.reshape(row_count, seq_count, kv_count, group_size, HEAD).transpose(
        1, 2, 3, 0, 4
    )
    q_heads = q_heads.reshape(seq_count, kv_count, group_size * row_count, HEAD)

    def stick_block(kv_block, bias_block, key_start):
        span_rows = kv_block.shape[0]
        key_pairs = kv_block.reshape(span_rows, seq_count, kv_count, 2 * HEAD)
        keys_part = key_pairs[..., :HEAD]
        values_part = key_pairs[..., HEAD:]
        scores = (
            jnp.einsum("bgmd,sbgd->bgms", q_heads, keys_part, preferred_element_type=jnp.float32)
            * 0.125
        )
        bias_float = jnp.transpose(bias_block, (1, 2, 0)).astype(jnp.float32)
        scores = (
            scores.reshape(seq_count, head_count, row_count, span_rows) + bias_float[:, :, None, :]
        )
        key_pos = key_start + lax.iota(jnp.int32, span_rows)
        strict = key_pos[None, :] < query_pos[:, None]
        log_pass = jnp.where(strict, jax.nn.log_sigmoid(-scores), 0.0)
        return (scores, strict, log_pass, values_part)

    def weigh(scores, strict, after_sum, values_part):
        span_rows = scores.shape[3]
        weights = jnp.where(strict, jnp.exp(jax.nn.log_sigmoid(scores) + after_sum), 0.0).astype(
            jnp.bfloat16
        )
        weights = weights.reshape(seq_count, kv_count, group_size * row_count, span_rows)
        return jnp.einsum(
            "bgms,sbgd->bgmd", weights, values_part, preferred_element_type=jnp.float32
        )

    empty_out = jnp.zeros((seq_count, kv_count, group_size * row_count, HEAD), jnp.float32)

    def sum_step(sums_table, kv_block, bias_block, key_start, shard_group):

        def sum_compute(table_in):
            scores, strict, log_pass, values_part = stick_block(kv_block, bias_block, key_start)
            block_sums = log_pass.reshape(
                seq_count, head_count, row_count, shard_group, row_count
            ).sum(axis=4)
            slot_index = key_start // row_count
            current = lax.dynamic_slice_in_dim(table_in, slot_index, shard_group, 0)
            return lax.dynamic_update_slice_in_dim(
                table_in, current + jnp.transpose(block_sums, (3, 0, 1, 2)), slot_index, 0
            )

        return lax.cond(
            key_start < query_start + row_count, sum_compute, lambda table_in: table_in, sums_table
        )

    empty_table = jnp.zeros((n_shards, seq_count, head_count, row_count), jnp.float32)
    sums_table = sweep_keys(
        empty_table,
        (
            lax.all_gather(key_values, "sp", axis=0, tiled=True),
            lax.all_gather(stop_bias, "sp", axis=0, tiled=True),
        ),
        row_count,
        sum_step,
    )
    offsets = lax.cumsum(sums_table, axis=0, reverse=True) - sums_table

    def out_step(outputs, kv_block, bias_block, key_start, shard_group):

        def out_compute(running):
            scores, strict, log_pass, values_part = stick_block(kv_block, bias_block, key_start)
            span_rows = kv_block.shape[0]
            split_pass = log_pass.reshape(seq_count, head_count, row_count, shard_group, row_count)
            within = lax.cumsum(split_pass, axis=4, reverse=True) - split_pass
            carried = lax.dynamic_slice_in_dim(offsets, key_start // row_count, shard_group, 0)
            carried = jnp.transpose(carried, (1, 2, 3, 0))[..., None]
            after_sum = (within + carried).reshape(seq_count, head_count, row_count, span_rows)
            return running + weigh(scores, strict, after_sum, values_part)

        return lax.cond(
            key_start < query_start + row_count, out_compute, lambda running: running, outputs
        )

    accum_out = sweep_keys(
        empty_out,
        (
            lax.all_gather(key_values, "sp", axis=0, tiled=True),
            lax.all_gather(stop_bias, "sp", axis=0, tiled=True),
        ),
        row_count,
        out_step,
    )
    attended = accum_out.reshape(seq_count, kv_count, group_size, row_count, HEAD).transpose(
        3, 0, 1, 2, 4
    )
    attended = attended.reshape(row_count * seq_count, head_count * HEAD).astype(jnp.bfloat16)
    share_tokens = row_count // lax.axis_size("tp")
    share_rows = share_tokens * seq_count
    tp_index = lax.axis_index("tp")
    projected = lax.psum(
        jnp.dot(attended, out_proj, preferred_element_type=jnp.float32).astype(jnp.bfloat16), "tp"
    ).astype(jnp.float32)
    flat_tokens = tokens.reshape(row_count * seq_count, tokens.shape[2])
    residual = (flat_tokens.astype(jnp.float32) + projected).astype(jnp.bfloat16)
    normed = rms_scale(residual, norm_gain)
    residual_share = lax.dynamic_slice_in_dim(residual, tp_index * share_rows, share_rows, 0)
    up_values = jnp.dot(
        normed,
        lax.all_gather(up_proj, "sp", axis=0, tiled=True),
        preferred_element_type=jnp.float32,
    )
    hidden = jnp.square(jax.nn.relu(up_values)).astype(jnp.bfloat16)
    partial_terms = jnp.dot(
        hidden,
        lax.all_gather(down_proj, "sp", axis=1, tiled=True),
        preferred_element_type=jnp.float32,
    )
    update = lax.psum_scatter(
        partial_terms.astype(jnp.bfloat16), "tp", scatter_dimension=0, tiled=True
    ).astype(jnp.float32)
    result = (residual_share.astype(jnp.float32) + update).astype(jnp.bfloat16)
    return result.reshape(share_tokens, seq_count, result.shape[1])


MESH = pl.DeviceIdType.MESH
LO = 4
LANES = 128
F32 = jnp.float32
BF16 = jnp.bfloat16


def remote(src, dst, send, recv, sp, tp):
    return pltpu.make_async_remote_copy(
        src_ref=src,
        dst_ref=dst,
        send_sem=send,
        recv_sem=recv,
        device_id={"sp": sp, "tp": tp},
        device_id_type=MESH,
    )


def dot_nt(a, b):
    return lax.dot_general(a, b, (((1,), (1,)), ((), ())), preferred_element_type=F32)


def dot_tn(a, b):
    return lax.dot_general(a, b, (((0,), (0,)), ((), ())), preferred_element_type=F32)


class Refs:
    def __init__(self, names, refs):
        for name, ref in zip(names, refs):
            setattr(self, name, ref)


class Piece:
    def __init__(self, r, place, view, rows, send, recv, half):
        self.r, self.view, self.rows, self.send, self.recv, self.half = r, view, rows, send, recv, half
        self.s, self.c, self.hi, self.lo, self.lo1, self.lo2, self.lo3 = place

    def full(self, j):
        return self.view(j, 0, self.rows)

    def part(self, j, h):
        return self.view(j, h * (self.rows // 2), self.rows // 2)

    def direct(self, z, src=None):
        j = z * LO + self.lo
        src = self.full(j) if src is None else src
        return [
            remote(src, self.full(j), self.send.at[z * 4 + k], self.recv.at[j], self.hi * LO + p, self.c)
            for k, p in enumerate((self.lo1, self.lo2))
        ]

    def diag(self, z):
        a, b = z * LO + self.lo1, z * LO + self.lo2
        first, last = self.part(a, 0), self.part(b, 1)
        return [
            remote(first, first, self.send.at[z * 4 + 2], self.recv.at[a], self.hi * LO + self.lo2, self.c),
            remote(last, last, self.send.at[z * 4 + 3], self.half.at[z], self.hi * LO + self.lo1, self.c),
        ]

    def arrived(self, ref, sem):
        remote(ref, ref, self.send.at[0], sem, self.s, 1 - self.c).wait_recv()

    def wait_own(self, z):
        j = z * LO + self.lo
        self.arrived(self.full(j), self.recv.at[j])

    def wait_direct(self, z):
        for p in (self.lo1, self.lo2):
            j = z * LO + p
            self.arrived(self.full(j), self.recv.at[j])

    def wait_diag(self, z):
        j = z * LO + self.lo3
        self.arrived(self.part(j, 0), self.recv.at[j])
        self.arrived(self.part(j, 1), self.half.at[z])


def start(copies):
    for copy in copies:
        copy.start()


def layer_kernel(HI, G, NC, names, *refs):
    r = Refs(names, refs)
    s = lax.axis_index("sp")
    c = lax.axis_index("tp")
    hi = s // LO
    lo = s % LO
    lo1 = lo + 1 - 2 * (lo % 2)
    lo2 = (lo + 2) % LO
    lo3 = (lo1 + 2) % LO
    other = 1 - c
    peers = (lo1, lo2, lo3)
    T = r.q_v.shape[0]
    H = T // 2
    D = r.tok_v.shape[1]
    R = r.up_v.shape[0]
    CH = r.up_buf.shape[1]
    W = r.dn_v.shape[1]
    PL = LO * T
    QR = 2 * PL
    own_cols = pl.ds(pl.multiple_of(hi * CH, LANES), CH)
    own_lanes = pl.ds(pl.multiple_of(lo * LANES, LANES), LANES)

    barrier = pltpu.get_barrier_semaphore()
    for p in peers:
        pl.semaphore_signal(barrier, inc=1, device_id={"sp": hi * LO + p, "tp": c}, device_id_type=MESH)
    pl.semaphore_signal(barrier, inc=1, device_id={"sp": s, "tp": other}, device_id_type=MESH)
    for dz in range(1, HI):
        far = ((hi + dz) % HI) * LO + lo
        pl.semaphore_signal(barrier, inc=1, device_id={"sp": far, "tp": c}, device_id_type=MESH)
    local = [
        (r.q_hbm, r.q_v),
        (r.kv_hbm, r.kv_v),
        (r.up_hbm, r.up_v),
        (r.dn_hbm, r.dn_v),
        (r.up_hbm.at[:, own_cols], r.up_buf.at[pl.ds(s * R, R)]),
        (r.dn_hbm.at[pl.ds(hi * CH, CH)], r.dn_buf.at[s]),
        (r.tok_hbm, r.tok_v),
        (r.wo_hbm, r.wo_v),
        (r.gain_hbm, r.gain_v),
    ]
    loads = [pltpu.make_async_copy(a, b, r.load_sem.at[i]) for i, (a, b) in enumerate(local)]
    start(loads)

    half_lane = lax.broadcasted_iota(jnp.int32, (2 * G, LANES), 1) // HEAD
    bias = r.bias_ref[...].astype(F32)
    bias = jnp.where(half_lane == lo % 2, jnp.concatenate([bias, bias], axis=1), 0.0)
    for g in range(G):
        r.bias_out[g] = bias if g == 0 else pltpu.roll(bias, 2 * G - 2 * g, 0)
    for load in loads[:4]:
        load.wait()
    pl.semaphore_wait(barrier, 4 + (HI - 1))

    place = (s, c, hi, lo, lo1, lo2, lo3)
    up = Piece(r, place, lambda j, a, n: r.up_buf.at[pl.ds(j * R + a, n)], R, r.up_sp, r.up_recv, r.up_half)
    dn = Piece(r, place, lambda j, a, n: r.dn_buf.at[j, pl.ds(a, n)], CH, r.dn_sp, r.dn_recv, r.dn_half)

    def arrived(ref, sem):
        remote(ref, ref, r.pj_send, sem, s, other).wait_recv()

    def spread_heads(k, p):
        lanes = pl.ds(pl.multiple_of(p * LANES, LANES), LANES)
        dev = hi * LO + p
        return [
            remote(r.kv_v.at[:, lanes], r.kv_buf.at[hi, pl.ds(lo * T, T)], r.a_send.at[3 * k], r.k_recv.at[lo], dev, c),
            remote(r.q_v.at[:, lanes], r.q_in.at[lo], r.a_send.at[3 * k + 1], r.q_recv.at[lo], dev, c),
            remote(r.bias_out.at[p], r.bias_in.at[lo], r.a_send.at[3 * k + 2], r.b_recv.at[lo], dev, c),
        ]

    def up_far(hp):
        cols = pl.ds(pl.multiple_of(hp * CH, LANES), CH)
        return remote(r.up_v.at[:, cols], up.full(s), r.wz_send.at[2 * hp], r.up_recv.at[s], hp * LO + lo, c)

    def dn_far(hp):
        rows = pl.ds(hp * CH, CH)
        return remote(r.dn_v.at[rows], dn.full(s), r.wz_send.at[2 * hp + 1], r.dn_recv.at[s], hp * LO + lo, c)

    small = jnp.minimum(hi, HI - 1 - hi)
    tilt = jnp.where(hi <= HI - 1 - hi, 1, -1)

    def nth(k):
        if k == 0:
            return hi
        near = hi - (k + 1) // 2 if k % 2 else hi + k // 2
        return jnp.where(k <= 2 * small, near, hi + tilt * (k - small))

    def below(far, d):
        @pl.when(hi >= d)
        def _():
            far(hi - d).start()

    def above(far, d):
        @pl.when(hi + d < HI)
        def _():
            far(hi + d).start()

    for k, p in enumerate(peers):
        start(spread_heads(k, p))
    start(up.direct(hi, r.up_v.at[:, own_cols]))
    start(dn.direct(hi, r.dn_v.at[pl.ds(hi * CH, CH)]))
    for d in range(1, HI):
        below(up_far, d)
    above(up_far, 1)

    r.q_in[lo] = r.q_v[:, own_lanes]
    r.kv_buf[hi, pl.ds(lo * T, T), :] = r.kv_v[:, own_lanes]
    r.bias_in[lo] = r.bias_out[lo]
    row_id = lax.broadcasted_iota(jnp.int32, (PL, PL + LANES), 0)
    col_id = lax.broadcasted_iota(jnp.int32, (PL, PL + LANES), 1)
    after_key = (row_id > col_id) | (col_id >= PL)
    r.tri_buf[...] = jnp.where(after_key, 1.0, 0.0).astype(BF16)
    low = lax.broadcasted_iota(jnp.int32, (T, LANES), 1) < HEAD

    for p in peers:
        arrived(r.kv_buf.at[hi, pl.ds(p * T, T)], r.k_recv.at[p])
        arrived(r.q_in.at[p], r.q_recv.at[p])
        arrived(r.bias_in.at[p], r.b_recv.at[p])
    for i in range(LO // 2):
        r.bias_pl[hi, :, i * LANES : (i + 1) * LANES] = r.bias_in[2 * i] + r.bias_in[2 * i + 1]

    def keys_up(z):
        dev = (hi + 1) * LO + lo
        return [
            remote(r.kv_buf.at[z], r.kv_buf.at[z], r.kz_send.at[2 * z], r.kz_recv.at[z], dev, c),
            remote(r.bias_pl.at[z], r.bias_pl.at[z], r.kz_send.at[2 * z + 1], r.bz_recv.at[z], dev, c),
        ]

    @pl.when(hi + 1 < HI)
    def _():
        start(keys_up(hi))

    for d in range(2, HI):
        above(up_far, d)

    for j in range(LO):
        qg = r.q_in[j].astype(F32) * 0.125
        r.q_all[j * T : (j + 1) * T] = jnp.where(low, qg, 0.0).astype(BF16)
        r.q_all[PL + j * T : PL + (j + 1) * T] = jnp.where(low, pltpu.roll(qg, HEAD, 1), 0.0).astype(BF16)

    step = 128

    def attend(z, own):
        keys = r.kv_buf[z]
        for i in range(QR // step):
            rows = slice(i * step, (i + 1) * step)
            head = i * step // PL
            scores = dot_nt(r.q_all[rows], keys) + r.bias_pl[z, head : head + 1, :]
            soft = jnp.maximum(scores, 0.0) + jnp.log(1.0 + jnp.exp(-jnp.abs(scores)))
            log_pass = -soft
            if own:
                query = i * step % PL + lax.broadcasted_iota(jnp.int32, (step, PL), 0)
                strict = lax.broadcasted_iota(jnp.int32, (step, PL), 1) < query
                log_pass = jnp.where(strict, log_pass, 0.0)
            top = log_pass.astype(BF16)
            rest = (log_pass - top.astype(F32)).astype(BF16)
            sums = jnp.dot(top, r.tri_buf[...], preferred_element_type=F32) + jnp.dot(
                rest, r.tri_buf[...], preferred_element_type=F32
            )
            power = scores - soft + sums[:, :PL]
            if not own:
                held = r.carry[rows]
                power = power + jnp.concatenate([held] * (PL // LANES), axis=1)
            weights = jnp.exp(power)
            if own:
                weights = jnp.where(strict, weights, 0.0)
            part = jnp.dot(weights.astype(BF16), keys, preferred_element_type=F32)
            if own:
                r.acc[rows] = part
                r.carry[rows] = sums[:, PL:]
            else:
                r.acc[rows] += part
                r.carry[rows] = held + sums[:, PL:]

    def look(d):
        @pl.when(hi >= d)
        def _():
            z = hi - d
            arrived(r.kv_buf.at[z], r.kz_recv.at[z])
            arrived(r.bias_pl.at[z], r.bz_recv.at[z])

            @pl.when(hi + 1 < HI)
            def _():
                start(keys_up(z))

            attend(z, False)

    def relay_direct(piece, k):
        piece.wait_own(nth(k))
        start(piece.direct(nth(k)))

    def relay_diag(piece, k):
        piece.wait_direct(nth(k))
        start(piece.diag(nth(k)))

    attend(hi, True)
    relay_diag(up, 0)
    relay_direct(up, 1)
    for d in range(1, HI):
        look(d)
        relay_diag(up, d)
        if d + 1 < HI:
            relay_direct(up, d + 1)

    heads = [r.acc[h * PL : (h + 1) * PL] for h in range(2)]
    low_pl = lax.broadcasted_iota(jnp.int32, (PL, LANES), 1) < HEAD
    r.att_pl[...] = jnp.where(low_pl, pltpu.roll(heads[0], HEAD, 1), heads[1]).astype(BF16)

    def att_back(k, p):
        src = r.att_pl.at[pl.ds(p * T, T)]
        return remote(src, r.att_buf.at[:, own_lanes], r.t_send.at[k], r.t_recv.at[lo], hi * LO + p, c)

    for k, p in enumerate(peers):
        att_back(k, p).start()
    r.att_buf[:, own_lanes] = r.att_pl[pl.ds(lo * T, T), :]
    relay_diag(dn, 0)
    for d in range(1, HI):
        below(dn_far, d)
        above(dn_far, d)
    for load in loads[4:]:
        load.wait()
    for p in peers:
        lanes = pl.ds(pl.multiple_of(p * LANES, LANES), LANES)
        arrived(r.att_buf.at[:, lanes], r.t_recv.at[p])

    att = r.att_buf[...]
    wide = 512 if D % 512 == 0 else LANES
    for i in range(D // wide):
        cols = slice(i * wide, (i + 1) * wide)
        r.pj_buf[:, cols] = jnp.dot(att, r.wo_v[:, cols], preferred_element_type=F32).astype(BF16)
    pj_copy = remote(r.pj_buf.at[pl.ds(other * H, H)], r.pj_in, r.pj_send, r.pj_recv, s, other)
    pj_copy.start()
    pj_copy.wait()
    mine = pl.ds(c * H, H)
    total = r.pj_buf[mine, :].astype(F32) + r.pj_in[...].astype(F32)
    residual = (r.tok_v[mine, :].astype(F32) + total).astype(BF16)
    r.res_buf[...] = residual
    values = residual.astype(F32)
    factor = lax.rsqrt(jnp.mean(values * values, axis=-1, keepdims=True) + EPSILON)
    r.n_buf[pl.ds((c * HI + hi) * H, H), :] = (values * factor * r.gain_v[...]).astype(BF16)

    NW = D // NC

    def n_at(z, core, q):
        return r.n_buf.at[pl.ds((core * HI + z) * H, H), q * NW : (q + 1) * NW]

    def n_up(z, q):
        return remote(n_at(z, c, q), n_at(z, c, q), r.nu_send.at[z * NC + q], r.nz_recv.at[z * NC + q], s + LO, c)

    def n_down(z, q):
        return remote(n_at(z, c, q), n_at(z, c, q), r.nd_send.at[z * NC + q], r.nz_recv.at[z * NC + q], s - LO, c)

    def n_pass(z, q):
        return remote(n_at(z, c, q), n_at(z, c, q), r.np_send.at[z * NC + q], r.nc_recv.at[z * NC + q], s, other)

    for q in range(NC):

        @pl.when(hi + 1 < HI)
        def _():
            n_up(hi, q).start()

        @pl.when(hi > 0)
        def _():
            n_down(hi, q).start()

    for q in range(NC):
        n_pass(hi, q).start()

    def norm_below(d):
        @pl.when(hi >= d)
        def _():
            z = hi - d
            for q in range(NC):
                arrived(n_at(z, c, q), r.nz_recv.at[z * NC + q])

                @pl.when(hi + 1 < HI)
                def _():
                    n_up(z, q).start()

                n_pass(z, q).start()

    def norm_above(d):
        @pl.when(hi + d < HI)
        def _():
            z = hi + d
            for q in range(NC):
                arrived(n_at(z, c, q), r.nz_recv.at[z * NC + q])

                @pl.when(hi > 0)
                def _():
                    n_down(z, q).start()

                n_pass(z, q).start()

    for d in range(1, HI):
        norm_below(d)
    relay_direct(dn, 1)
    for d in range(1, HI):
        norm_above(d)
        if d == 1:
            relay_diag(dn, 1)
            relay_direct(dn, 2)
    for z in range(HI):
        for q in range(NC):
            arrived(n_at(z, other, q), r.nc_recv.at[z * NC + q])
    for k in range(HI):
        up.wait_diag(nth(k))
    relay_diag(dn, 2)

    wide = 256 if CH % 256 == 0 else LANES
    for i in range(CH // wide):
        cols = slice(i * wide, (i + 1) * wide)
        raw = jnp.maximum(jnp.dot(r.n_buf[...], r.up_buf[:, cols], preferred_element_type=F32), 0.0)
        r.hid_buf[:, cols] = (raw * raw).astype(BF16)
    for k in range(3, HI):
        relay_direct(dn, k)

    half = HI * H

    def x_out(k):
        z = nth(k)
        rows = pl.ds(other * half, half)
        return remote(r.ps_buf.at[z, rows], r.x_in.at[z], r.x_send.at[k], r.x_recv.at[z], s, other)

    def p_out(k, far):
        z = nth(k)
        hp = (hi + far) % HI
        return remote(
            r.xs_buf.at[z, pl.ds(hp * H, H)],
            r.pr_buf.at[hi, z],
            r.p_send.at[k * HI + far],
            r.p_recv.at[hi * HI + z],
            hp * LO + lo,
            c,
        )

    def spread(k):
        z = nth(k)
        arrived(r.x_in.at[z], r.x_recv.at[z])
        mixed = r.ps_buf[z, pl.ds(c * half, half), :].astype(F32) + r.x_in[z].astype(F32)
        r.xs_buf[z] = mixed.astype(BF16)
        for far in range(1, HI):
            p_out(k, far).start()

    for k in range(HI):
        if k >= 2 and k + 1 < HI:
            relay_diag(dn, k + 1)
        z = nth(k)
        dn.wait_diag(z)
        for q in range(0, LO, 2):
            pair = jnp.concatenate([r.dn_buf[z * LO + q], r.dn_buf[z * LO + q + 1]], axis=1)
            part = jnp.dot(r.hid_buf[...], pair, preferred_element_type=F32)
            r.ps_buf[z, :, q * W : (q + 2) * W] = part.astype(BF16)
        x_out(k).start()
        if k > 0:
            spread(k - 1)
    spread(HI - 1)
    CW = LO * W
    for k in range(HI):
        z = nth(k)
        cols = pl.ds(pl.multiple_of(z * CW, LANES), CW)
        update = r.xs_buf[z, pl.ds(hi * H, H), :].astype(F32)
        for far in range(1, HI):
            src = (hi + HI - far) % HI
            arrived(r.pr_buf.at[src, z], r.p_recv.at[src * HI + z])
            update = update + r.pr_buf[src, z].astype(F32)
        r.out_ref[:, cols] = (r.res_buf[:, cols].astype(F32) + update).astype(BF16)

    for k, p in enumerate(peers):
        for copy in spread_heads(k, p):
            copy.wait_send()
        att_back(k, p).wait_send()
    for z in range(HI):

        @pl.when(z != hi)
        def _():
            up_far(z).wait_send()
            dn_far(z).wait_send()

        for copy in up.direct(z) + up.diag(z) + dn.direct(z) + dn.diag(z):
            copy.wait_send()

        @pl.when((z <= hi) & (hi + 1 < HI))
        def _():
            for copy in keys_up(z):
                copy.wait_send()
            for q in range(NC):
                n_up(z, q).wait_send()

        @pl.when((z >= hi) & (hi > 0))
        def _():
            for q in range(NC):
                n_down(z, q).wait_send()

        for q in range(NC):
            n_pass(z, q).wait_send()
        x_out(z).wait_send()
        for far in range(1, HI):
            p_out(z, far).wait_send()


def fits(tokens, queries, key_values, stop_bias, up_proj, down_proj):
    sp = lax.axis_size("sp")
    rows, seqs, heads = stop_bias.shape
    hidden = up_proj.shape[1]
    return (
        lax.axis_size("tp") == 2
        and sp % LO == 0
        and sp > LO
        and seqs == 1
        and heads == 2 * LO
        and queries.shape[2] == heads * HEAD
        and key_values.shape[2] == heads * HEAD
        and 2 * HEAD == LANES
        and 2 * rows == LANES
        and hidden % (sp // LO * LANES) == 0
        and down_proj.shape[1] % LANES == 0
        and up_proj.shape[0] % 16 == 0
        and tokens.shape[2] % 512 == 0
    )


def body(tokens, queries, key_values, stop_bias, out_proj, norm_gain, up_proj, down_proj):
    if not fits(tokens, queries, key_values, stop_bias, up_proj, down_proj):
        return general_body(
            tokens, queries, key_values, stop_bias, out_proj, norm_gain, up_proj, down_proj
        )
    sp = lax.axis_size("sp")
    HI = sp // LO
    T, _, D = tokens.shape
    H = T // 2
    heads = stop_bias.shape[2]
    G = heads // 2
    R, hidden = up_proj.shape
    CH = hidden // HI
    W = down_proj.shape[1]
    PL = LO * T
    NC = 4
    vmem = pl.BlockSpec(memory_space=pltpu.VMEM)
    hbm = pl.BlockSpec(memory_space=pl.ANY)

    def sem(*shape):
        return pltpu.SemaphoreType.DMA(shape)

    operands = dict(
        tok_hbm=(tokens.reshape(T, D), hbm),
        q_hbm=(queries.reshape(T, queries.shape[2]), hbm),
        kv_hbm=(key_values.reshape(T, key_values.shape[2]), hbm),
        bias_ref=(stop_bias.reshape(T, heads).T, vmem),
        wo_hbm=(out_proj, hbm),
        gain_hbm=(norm_gain.reshape(1, D), hbm),
        up_hbm=(up_proj, hbm),
        dn_hbm=(down_proj, hbm),
    )
    scratch = dict(
        tok_v=pltpu.VMEM((T, D), BF16),
        q_v=pltpu.VMEM((T, G * LANES), BF16),
        kv_v=pltpu.VMEM((T, G * LANES), BF16),
        wo_v=pltpu.VMEM(out_proj.shape, BF16),
        gain_v=pltpu.VMEM((1, D), F32),
        up_v=pltpu.VMEM((R, hidden), BF16),
        dn_v=pltpu.VMEM((hidden, W), BF16),
        up_buf=pltpu.VMEM((sp * R, CH), BF16),
        dn_buf=pltpu.VMEM((sp, CH, W), BF16),
        bias_out=pltpu.VMEM((G, 2 * G, LANES), F32),
        bias_in=pltpu.VMEM((LO, 2 * G, LANES), F32),
        bias_pl=pltpu.VMEM((HI, 2 * G, PL), F32),
        q_in=pltpu.VMEM((LO, T, LANES), BF16),
        q_all=pltpu.VMEM((2 * PL, LANES), BF16),
        kv_buf=pltpu.VMEM((HI, PL, LANES), BF16),
        tri_buf=pltpu.VMEM((PL, PL + LANES), BF16),
        carry=pltpu.VMEM((2 * PL, LANES), F32),
        acc=pltpu.VMEM((2 * PL, LANES), F32),
        att_pl=pltpu.VMEM((PL, LANES), BF16),
        att_buf=pltpu.VMEM((T, G * LANES), BF16),
        pj_buf=pltpu.VMEM((T, D), BF16),
        pj_in=pltpu.VMEM((H, D), BF16),
        res_buf=pltpu.VMEM((H, D), BF16),
        n_buf=pltpu.VMEM((HI * T, D), BF16),
        hid_buf=pltpu.VMEM((HI * T, CH), BF16),
        ps_buf=pltpu.VMEM((HI, HI * T, LO * W), BF16),
        x_in=pltpu.VMEM((HI, HI * H, LO * W), BF16),
        xs_buf=pltpu.VMEM((HI, HI * H, LO * W), BF16),
        pr_buf=pltpu.VMEM((HI, HI, H, LO * W), BF16),
        load_sem=sem(9),
        a_send=sem(9),
        k_recv=sem(LO),
        q_recv=sem(LO),
        b_recv=sem(LO),
        kz_send=sem(2 * HI),
        kz_recv=sem(HI),
        bz_recv=sem(HI),
        wz_send=sem(HI * 2),
        up_sp=sem(HI * 4),
        up_recv=sem(sp),
        up_half=sem(HI),
        dn_sp=sem(HI * 4),
        dn_recv=sem(sp),
        dn_half=sem(HI),
        t_send=sem(3),
        t_recv=sem(LO),
        pj_send=pltpu.SemaphoreType.DMA,
        pj_recv=pltpu.SemaphoreType.DMA,
        nu_send=sem(HI * NC),
        nd_send=sem(HI * NC),
        np_send=sem(HI * NC),
        nz_recv=sem(HI * NC),
        nc_recv=sem(HI * NC),
        x_send=sem(HI),
        x_recv=sem(HI),
        p_send=sem(HI * HI),
        p_recv=sem(HI * HI),
    )
    names = [*operands, "out_ref", *scratch]
    out = pl.pallas_call(
        lambda *refs: layer_kernel(HI, G, NC, names, *refs),
        out_shape=jax.ShapeDtypeStruct((H, D), BF16),
        in_specs=[spec for _, spec in operands.values()],
        out_specs=vmem,
        scratch_shapes=list(scratch.values()),
        compiler_params=pltpu.CompilerParams(
            collective_id=0, has_side_effects=True, vmem_limit_bytes=56 * 1024 * 1024
        ),
        name="layer",
    )(*[value for value, _ in operands.values()])
    return out.reshape(H, 1, D)


def solution(mesh):
    return jax.shard_map(
        body,
        mesh=mesh,
        in_specs=(
            P("sp", None, None),
            P("sp", None, "tp"),
            P("sp", None, "tp"),
            P("sp", None, "tp"),
            P("tp", None),
            P(),
            P("sp", "tp"),
            P("tp", "sp"),
        ),
        out_specs=P(("sp", "tp"), None, None),
        check_vma=False,
    )
```

time: 74.3 us -> 78.7 us (1.059)
  Pallas kernels: 71.1 us -> 77 us
  local copies, waits for them, and re-layouts: 2.94 us -> 1.57 us
    pallas_call x1, Pallas kernels: 71.1 us -> 77 us  [body(): pl.pallas_call(lambda *refs: layer_kernel(HI, G, NC, names, *refs), out_s...]
    unnamed x2 -> x1, local copies, waits for them, and re-layouts: 2.94 us -> 1.57 us
where the time goes in v1:
time: 78.7 us; the launch traced here: 78.5 us
  Pallas kernels  77 us (98%)
  local copies, waits for them, and re-layouts  1.57 us (2%)
    pallas_call x1, Pallas kernels, body(): pl.pallas_call(lambda *refs: layer_kernel(HI, G, NC, names, *refs), out_s...  77 us

profile of v1, /device:TPU:0, one launch (start us, length us, event | category | flops | bytes accessed | tf_op | source)
XLA Modules:
  0.0 78.5 jit_solution(11047928078171465454)
XLA Ops:
  0.0 77.0 %layer.1 = bf16[32,2048]{1,0:T(8,128)(2,1)} custom-call(bf16[64,2048]{1,0:T(8,128)(2,1)} %bitcast.9, bf16[64,512]{1,0:T(8,128)(2,1)} %bitcast.10, bf16[64,512]{1,0:T(8,128)(2,1)} %bitcast.11, bf16[8,64]{1,0:T(8,128)(2,1)} %bitcast.13, bf16[512,2048]{1,0:T(8,128)(2,1)} %refs_4_.1, f32[1,2048]{1,0:T(1,128)} %bitcast.12, bf16[128,2048]{1,0:T(8,128)(2,1)} %refs_6_.1, ...), custom_call_target="tpu_custom_call" | custom-call | tf_op jit(solution)/shard_map/layer/pallas_call | solution.py:761
  77.0 1.6 %copy.10 = bf16[32,1,2048]{2,0,1:T(8,128)(2,1)} copy(bf16[32,1,2048]{2,0,1:T(8,128)(2,1)} %bitcast.8) | data formatting | bytes 262144

commit v2 on v1

--- a/solution.py
+++ b/solution.py
@@ -197,8 +197,9 @@
 
 
 class Piece:
-    def __init__(self, r, place, view, rows, send, recv, half):
-        self.r, self.view, self.rows, self.send, self.recv, self.half = r, view, rows, send, recv, half
+    def __init__(self, place, view, blocks, rows, sem):
+        self.view, self.blocks, self.rows = view, blocks, rows
+        self.send, self.own, self.near, self.far = sem
         self.s, self.c, self.hi, self.lo, self.lo1, self.lo2, self.lo3 = place
 
     def full(self, j):
@@ -211,39 +212,42 @@
         j = z * LO + self.lo
         src = self.full(j) if src is None else src
         return [
-            remote(src, self.full(j), self.send.at[z * 4 + k], self.recv.at[j], self.hi * LO + p, self.c)
-            for k, p in enumerate((self.lo1, self.lo2))
+            remote(src, self.full(j), self.send.at[0], self.near.at[z], self.hi * LO + p, self.c)
+            for p in (self.lo1, self.lo2)
         ]
 
     def diag(self, z):
-        a, b = z * LO + self.lo1, z * LO + self.lo2
-        first, last = self.part(a, 0), self.part(b, 1)
+        first, last = self.part(z * LO + self.lo1, 0), self.part(z * LO + self.lo2, 1)
         return [
-            remote(first, first, self.send.at[z * 4 + 2], self.recv.at[a], self.hi * LO + self.lo2, self.c),
-            remote(last, last, self.send.at[z * 4 + 3], self.half.at[z], self.hi * LO + self.lo1, self.c),
+            remote(first, first, self.send.at[0], self.far.at[z], self.hi * LO + self.lo2, self.c),
+            remote(last, last, self.send.at[0], self.far.at[z], self.hi * LO + self.lo1, self.c),
         ]
 
     def arrived(self, ref, sem):
         remote(ref, ref, self.send.at[0], sem, self.s, 1 - self.c).wait_recv()
 
     def wait_own(self, z):
-        j = z * LO + self.lo
-        self.arrived(self.full(j), self.recv.at[j])
+        self.arrived(self.full(z * LO + self.lo), self.own.at[z])
 
     def wait_direct(self, z):
-        for p in (self.lo1, self.lo2):
-            j = z * LO + p
-            self.arrived(self.full(j), self.recv.at[j])
+        self.arrived(self.blocks(2), self.near.at[z])
 
     def wait_diag(self, z):
-        j = z * LO + self.lo3
-        self.arrived(self.part(j, 0), self.recv.at[j])
-        self.arrived(self.part(j, 1), self.half.at[z])
+        self.arrived(self.full(z * LO + self.lo3), self.far.at[z])
+
+    def wait_sent(self, planes):
+        ref = self.blocks(3 * planes)
+        remote(ref, ref, self.send.at[0], self.far.at[0], self.s, 1 - self.c).wait_send()
 
 
 def start(copies):
     for copy in copies:
         copy.start()
+
+
+def scoped(name, fn, *args):
+    with jax.named_scope(name):
+        return fn(*args)
 
 
 def layer_kernel(HI, G, NC, names, *refs):
@@ -276,8 +280,9 @@
         far = ((hi + dz) % HI) * LO + lo
         pl.semaphore_signal(barrier, inc=1, device_id={"sp": far, "tp": c}, device_id_type=MESH)
     local = [
+        (r.bias_hbm, r.bias_v),
+        (r.kv_hbm, r.kv_v),
         (r.q_hbm, r.q_v),
-        (r.kv_hbm, r.kv_v),
         (r.up_hbm, r.up_v),
         (r.dn_hbm, r.dn_v),
         (r.up_hbm.at[:, own_cols], r.up_buf.at[pl.ds(s * R, R)]),
@@ -288,39 +293,67 @@
     ]
     loads = [pltpu.make_async_copy(a, b, r.load_sem.at[i]) for i, (a, b) in enumerate(local)]
     start(loads)
+    loads[0].wait()
 
     half_lane = lax.broadcasted_iota(jnp.int32, (2 * G, LANES), 1) // HEAD
-    bias = r.bias_ref[...].astype(F32)
+    bias = r.bias_v[...].astype(F32)
     bias = jnp.where(half_lane == lo % 2, jnp.concatenate([bias, bias], axis=1), 0.0)
     for g in range(G):
-        r.bias_out[g] = bias if g == 0 else pltpu.roll(bias, 2 * G - 2 * g, 0)
-    for load in loads[:4]:
-        load.wait()
-    pl.semaphore_wait(barrier, 4 + (HI - 1))
+        r.bias_out[g] = bias[2 * g : 2 * g + 2]
+    with jax.named_scope("barrier"):
+        for load in loads[1:5]:
+            load.wait()
+        pl.semaphore_wait(barrier, 4 + (HI - 1))
 
     place = (s, c, hi, lo, lo1, lo2, lo3)
-    up = Piece(r, place, lambda j, a, n: r.up_buf.at[pl.ds(j * R + a, n)], R, r.up_sp, r.up_recv, r.up_half)
-    dn = Piece(r, place, lambda j, a, n: r.dn_buf.at[j, pl.ds(a, n)], CH, r.dn_sp, r.dn_recv, r.dn_half)
+    up = Piece(
+        place,
+        lambda j, a, n: r.up_buf.at[pl.ds(j * R + a, n)],
+        lambda n: r.up_buf.at[pl.ds(0, n * R)],
+        R,
+        (r.up_sp, r.up_own, r.up_near, r.up_diag),
+    )
+    dn = Piece(
+        place,
+        lambda j, a, n: r.dn_buf.at[j, pl.ds(a, n)],
+        lambda n: r.dn_buf.at[pl.ds(0, n)],
+        CH,
+        (r.dn_sp, r.dn_own, r.dn_near, r.dn_diag),
+    )
 
     def arrived(ref, sem):
         remote(ref, ref, r.pj_send, sem, s, other).wait_recv()
 
-    def spread_heads(k, p):
+    def sent(ref, sem):
+        remote(ref, ref, sem, r.pj_recv, s, other).wait_send()
+
+    def send_keys(d, p):
         lanes = pl.ds(pl.multiple_of(p * LANES, LANES), LANES)
-        dev = hi * LO + p
+        dev = (hi + d) * LO + p
         return [
-            remote(r.kv_v.at[:, lanes], r.kv_buf.at[hi, pl.ds(lo * T, T)], r.a_send.at[3 * k], r.k_recv.at[lo], dev, c),
-            remote(r.q_v.at[:, lanes], r.q_in.at[lo], r.a_send.at[3 * k + 1], r.q_recv.at[lo], dev, c),
-            remote(r.bias_out.at[p], r.bias_in.at[lo], r.a_send.at[3 * k + 2], r.b_recv.at[lo], dev, c),
+            remote(r.kv_v.at[:, lanes], r.kv_buf.at[hi, pl.ds(lo * T, T)], r.k_send.at[d], r.k_recv.at[hi], dev, c),
+            remote(r.bias_out.at[p], r.bias_in.at[hi, lo], r.b_send.at[d], r.b_recv.at[hi], dev, c),
         ]
+
+    def send_queries(p):
+        lanes = pl.ds(pl.multiple_of(p * LANES, LANES), LANES)
+        return remote(r.q_v.at[:, lanes], r.q_in.at[lo], r.q_send.at[0], r.q_recv.at[0], hi * LO + p, c)
+
+    def keys_of(z, shards):
+        arrived(r.kv_buf.at[z, pl.ds(0, shards * T)], r.k_recv.at[z])
+        arrived(r.bias_in.at[z, pl.ds(0, shards)], r.b_recv.at[z])
+
+    def join_bias(z):
+        for i in range(LO // 2):
+            r.bias_pl[z, :, i * LANES : (i + 1) * LANES] = r.bias_in[z, 2 * i] + r.bias_in[z, 2 * i + 1]
 
     def up_far(hp):
         cols = pl.ds(pl.multiple_of(hp * CH, LANES), CH)
-        return remote(r.up_v.at[:, cols], up.full(s), r.wz_send.at[2 * hp], r.up_recv.at[s], hp * LO + lo, c)
+        return remote(r.up_v.at[:, cols], up.full(s), r.wz_send.at[0], r.up_own.at[hi], hp * LO + lo, c)
 
     def dn_far(hp):
         rows = pl.ds(hp * CH, CH)
-        return remote(r.dn_v.at[rows], dn.full(s), r.wz_send.at[2 * hp + 1], r.dn_recv.at[s], hp * LO + lo, c)
+        return remote(r.dn_v.at[rows], dn.full(s), r.wz_send.at[1], r.dn_own.at[hi], hp * LO + lo, c)
 
     small = jnp.minimum(hi, HI - 1 - hi)
     tilt = jnp.where(hi <= HI - 1 - hi, 1, -1)
@@ -328,7 +361,7 @@
     def nth(k):
         if k == 0:
             return hi
-        near = hi - (k + 1) // 2 if k % 2 else hi + k // 2
+        near = hi + (k + 1) // 2 if k % 2 else hi - k // 2
         return jnp.where(k <= 2 * small, near, hi + tilt * (k - small))
 
     def below(far, d):
@@ -341,44 +374,43 @@
         def _():
             far(hi + d).start()
 
-    for k, p in enumerate(peers):
-        start(spread_heads(k, p))
-    start(up.direct(hi, r.up_v.at[:, own_cols]))
-    start(dn.direct(hi, r.dn_v.at[pl.ds(hi * CH, CH)]))
+    for p in peers:
+        pl.semaphore_signal(r.ready, inc=1, device_id={"sp": hi * LO + p, "tp": c}, device_id_type=MESH)
+    for p in peers:
+        start(send_keys(0, p))
+        send_queries(p).start()
+
+    def raise_keys(shards):
+        for d in range(HI - 1, 0, -1):
+
+            @pl.when(hi + d < HI)
+            def _():
+                for p in shards:
+                    start(send_keys(d, p))
+
+    raise_keys((lo,))
     for d in range(1, HI):
         below(up_far, d)
-    above(up_far, 1)
+    scoped("ready", pl.semaphore_wait, r.ready, LO - 1)
+    raise_keys(peers)
+    start(up.direct(hi, r.up_v.at[:, own_cols]))
+    for d in range(1, HI):
+        above(up_far, d)
+    start(dn.direct(hi, r.dn_v.at[pl.ds(hi * CH, CH)]))
 
     r.q_in[lo] = r.q_v[:, own_lanes]
     r.kv_buf[hi, pl.ds(lo * T, T), :] = r.kv_v[:, own_lanes]
-    r.bias_in[lo] = r.bias_out[lo]
+    r.bias_in[hi, lo] = r.bias_out[lo]
     row_id = lax.broadcasted_iota(jnp.int32, (PL, PL + LANES), 0)
     col_id = lax.broadcasted_iota(jnp.int32, (PL, PL + LANES), 1)
     after_key = (row_id > col_id) | (col_id >= PL)
     r.tri_buf[...] = jnp.where(after_key, 1.0, 0.0).astype(BF16)
     low = lax.broadcasted_iota(jnp.int32, (T, LANES), 1) < HEAD
 
-    for p in peers:
-        arrived(r.kv_buf.at[hi, pl.ds(p * T, T)], r.k_recv.at[p])
-        arrived(r.q_in.at[p], r.q_recv.at[p])
-        arrived(r.bias_in.at[p], r.b_recv.at[p])
-    for i in range(LO // 2):
-        r.bias_pl[hi, :, i * LANES : (i + 1) * LANES] = r.bias_in[2 * i] + r.bias_in[2 * i + 1]
-
-    def keys_up(z):
-        dev = (hi + 1) * LO + lo
-        return [
-            remote(r.kv_buf.at[z], r.kv_buf.at[z], r.kz_send.at[2 * z], r.kz_recv.at[z], dev, c),
-            remote(r.bias_pl.at[z], r.bias_pl.at[z], r.kz_send.at[2 * z + 1], r.bz_recv.at[z], dev, c),
-        ]
-
-    @pl.when(hi + 1 < HI)
-    def _():
-        start(keys_up(hi))
-
-    for d in range(2, HI):
-        above(up_far, d)
-
+    with jax.named_scope("heads_wait"):
+        keys_of(hi, LO - 1)
+        arrived(r.q_in.at[pl.ds(0, LO - 1)], r.q_recv.at[0])
+    join_bias(hi)
     for j in range(LO):
         qg = r.q_in[j].astype(F32) * 0.125
         r.q_all[j * T : (j + 1) * T] = jnp.where(low, qg, 0.0).astype(BF16)
@@ -422,52 +454,44 @@
         @pl.when(hi >= d)
         def _():
             z = hi - d
-            arrived(r.kv_buf.at[z], r.kz_recv.at[z])
-            arrived(r.bias_pl.at[z], r.bz_recv.at[z])
-
-            @pl.when(hi + 1 < HI)
-            def _():
-                start(keys_up(z))
-
-            attend(z, False)
+            scoped(f"keys_wait{d}", keys_of, z, LO)
+            join_bias(z)
+            scoped(f"attend{d}", attend, z, False)
 
     def relay_direct(piece, k):
-        piece.wait_own(nth(k))
+        scoped(f"own_wait{k}", piece.wait_own, nth(k))
         start(piece.direct(nth(k)))
 
     def relay_diag(piece, k):
-        piece.wait_direct(nth(k))
+        scoped(f"direct_wait{k}", piece.wait_direct, nth(k))
         start(piece.diag(nth(k)))
 
-    attend(hi, True)
+    scoped("attend0", attend, hi, True)
     relay_diag(up, 0)
-    relay_direct(up, 1)
     for d in range(1, HI):
         look(d)
-        relay_diag(up, d)
-        if d + 1 < HI:
-            relay_direct(up, d + 1)
+        if d == 1:
+            relay_direct(up, 1)
 
     heads = [r.acc[h * PL : (h + 1) * PL] for h in range(2)]
     low_pl = lax.broadcasted_iota(jnp.int32, (PL, LANES), 1) < HEAD
     r.att_pl[...] = jnp.where(low_pl, pltpu.roll(heads[0], HEAD, 1), heads[1]).astype(BF16)
 
-    def att_back(k, p):
+    def att_back(p):
         src = r.att_pl.at[pl.ds(p * T, T)]
-        return remote(src, r.att_buf.at[:, own_lanes], r.t_send.at[k], r.t_recv.at[lo], hi * LO + p, c)
-
-    for k, p in enumerate(peers):
-        att_back(k, p).start()
-    r.att_buf[:, own_lanes] = r.att_pl[pl.ds(lo * T, T), :]
-    relay_diag(dn, 0)
+        return remote(src, r.att_buf.at[:, own_lanes], r.t_send.at[0], r.t_recv.at[0], hi * LO + p, c)
+
+    for p in peers:
+        att_back(p).start()
     for d in range(1, HI):
         below(dn_far, d)
         above(dn_far, d)
-    for load in loads[4:]:
-        load.wait()
-    for p in peers:
-        lanes = pl.ds(pl.multiple_of(p * LANES, LANES), LANES)
-        arrived(r.att_buf.at[:, lanes], r.t_recv.at[p])
+    relay_diag(dn, 0)
+    r.att_buf[:, own_lanes] = r.att_pl[pl.ds(lo * T, T), :]
+    with jax.named_scope("att_wait"):
+        for load in loads[5:]:
+            load.wait()
+        arrived(r.att_pl.at[pl.ds(0, (LO - 1) * T)], r.t_recv.at[0])
 
     att = r.att_buf[...]
     wide = 512 if D % 512 == 0 else LANES
@@ -476,7 +500,9 @@
         r.pj_buf[:, cols] = jnp.dot(att, r.wo_v[:, cols], preferred_element_type=F32).astype(BF16)
     pj_copy = remote(r.pj_buf.at[pl.ds(other * H, H)], r.pj_in, r.pj_send, r.pj_recv, s, other)
     pj_copy.start()
-    pj_copy.wait()
+    relay_direct(up, 2)
+    relay_diag(up, 1)
+    scoped("pj_wait", pj_copy.wait)
     mine = pl.ds(c * H, H)
     total = r.pj_buf[mine, :].astype(F32) + r.pj_in[...].astype(F32)
     residual = (r.tok_v[mine, :].astype(F32) + total).astype(BF16)
@@ -491,13 +517,13 @@
         return r.n_buf.at[pl.ds((core * HI + z) * H, H), q * NW : (q + 1) * NW]
 
     def n_up(z, q):
-        return remote(n_at(z, c, q), n_at(z, c, q), r.nu_send.at[z * NC + q], r.nz_recv.at[z * NC + q], s + LO, c)
+        return remote(n_at(z, c, q), n_at(z, c, q), r.nu_send.at[z], r.nz_recv.at[z * NC + q], s + LO, c)
 
     def n_down(z, q):
-        return remote(n_at(z, c, q), n_at(z, c, q), r.nd_send.at[z * NC + q], r.nz_recv.at[z * NC + q], s - LO, c)
+        return remote(n_at(z, c, q), n_at(z, c, q), r.nd_send.at[z], r.nz_recv.at[z * NC + q], s - LO, c)
 
     def n_pass(z, q):
-        return remote(n_at(z, c, q), n_at(z, c, q), r.np_send.at[z * NC + q], r.nc_recv.at[z * NC + q], s, other)
+        return remote(n_at(z, c, q), n_at(z, c, q), r.np_send.at[0], r.nc_recv.at[0], s, other)
 
     for q in range(NC):
 
@@ -512,87 +538,74 @@
     for q in range(NC):
         n_pass(hi, q).start()
 
-    def norm_below(d):
-        @pl.when(hi >= d)
-        def _():
-            z = hi - d
-            for q in range(NC):
-                arrived(n_at(z, c, q), r.nz_recv.at[z * NC + q])
-
-                @pl.when(hi + 1 < HI)
-                def _():
-                    n_up(z, q).start()
-
-                n_pass(z, q).start()
-
-    def norm_above(d):
-        @pl.when(hi + d < HI)
-        def _():
-            z = hi + d
-            for q in range(NC):
-                arrived(n_at(z, c, q), r.nz_recv.at[z * NC + q])
-
-                @pl.when(hi > 0)
-                def _():
-                    n_down(z, q).start()
-
-                n_pass(z, q).start()
-
-    for d in range(1, HI):
-        norm_below(d)
+    upper = hi // (HI // 2)
+
+    def norm_take(k):
+        rank = hi + upper * (HI - 1 - 2 * hi)
+        z = k - 1 + (rank < k).astype(jnp.int32)
+        z = z + upper * (HI - 1 - 2 * z)
+        for q in range(NC):
+            scoped(f"norm_wait{k}", arrived, n_at(z, c, q), r.nz_recv.at[z * NC + q])
+
+            @pl.when((z < hi) & (hi + 1 < HI))
+            def _():
+                n_up(z, q).start()
+
+            @pl.when((z > hi) & (hi > 0))
+            def _():
+                n_down(z, q).start()
+
+            n_pass(z, q).start()
+
+    for k in range(3, HI):
+        relay_direct(up, k)
+        relay_diag(up, k - 1)
     relay_direct(dn, 1)
-    for d in range(1, HI):
-        norm_above(d)
-        if d == 1:
-            relay_diag(dn, 1)
-            relay_direct(dn, 2)
-    for z in range(HI):
-        for q in range(NC):
-            arrived(n_at(z, other, q), r.nc_recv.at[z * NC + q])
-    for k in range(HI):
-        up.wait_diag(nth(k))
-    relay_diag(dn, 2)
+    for k in range(1, HI):
+        norm_take(k)
+        if k == 1:
+            relay_diag(up, HI - 1)
+        else:
+            relay_diag(dn, k - 1)
+        if k + 1 < HI:
+            relay_direct(dn, k + 1)
+    with jax.named_scope("norm_other_wait"):
+        arrived(r.n_buf.at[pl.ds(0, HI * H)], r.nc_recv.at[0])
+    with jax.named_scope("up_wait"):
+        for k in range(HI):
+            up.wait_diag(nth(k))
 
     wide = 256 if CH % 256 == 0 else LANES
     for i in range(CH // wide):
         cols = slice(i * wide, (i + 1) * wide)
         raw = jnp.maximum(jnp.dot(r.n_buf[...], r.up_buf[:, cols], preferred_element_type=F32), 0.0)
         r.hid_buf[:, cols] = (raw * raw).astype(BF16)
-    for k in range(3, HI):
-        relay_direct(dn, k)
-
     half = HI * H
+    CW = LO * W
+    mine_rows = pl.ds(c * half, half)
 
     def x_out(k):
         z = nth(k)
         rows = pl.ds(other * half, half)
-        return remote(r.ps_buf.at[z, rows], r.x_in.at[z], r.x_send.at[k], r.x_recv.at[z], s, other)
-
-    def p_out(k, far):
-        z = nth(k)
+        return remote(r.ps_buf.at[z, rows], r.x_in.at[z], r.x_send.at[0], r.x_recv.at[z], s, other)
+
+    def p_out(z, far):
         hp = (hi + far) % HI
-        return remote(
-            r.xs_buf.at[z, pl.ds(hp * H, H)],
-            r.pr_buf.at[hi, z],
-            r.p_send.at[k * HI + far],
-            r.p_recv.at[hi * HI + z],
-            hp * LO + lo,
-            c,
-        )
+        return remote(r.xs_buf.at[z, pl.ds(hp * H, H)], r.pr_buf.at[z, hi], r.p_send.at[0], r.p_recv.at[z], hp * LO + lo, c)
 
     def spread(k):
         z = nth(k)
-        arrived(r.x_in.at[z], r.x_recv.at[z])
-        mixed = r.ps_buf[z, pl.ds(c * half, half), :].astype(F32) + r.x_in[z].astype(F32)
+        scoped(f"x_wait{k}", arrived, r.x_in.at[z], r.x_recv.at[z])
+        mixed = r.ps_buf[z, mine_rows, :].astype(F32) + r.x_in[z].astype(F32)
         r.xs_buf[z] = mixed.astype(BF16)
+
         for far in range(1, HI):
-            p_out(k, far).start()
-
+            p_out(z, far).start()
+
+    relay_diag(dn, HI - 1)
     for k in range(HI):
-        if k >= 2 and k + 1 < HI:
-            relay_diag(dn, k + 1)
         z = nth(k)
-        dn.wait_diag(z)
+        scoped(f"dn_wait{k}", dn.wait_diag, z)
         for q in range(0, LO, 2):
             pair = jnp.concatenate([r.dn_buf[z * LO + q], r.dn_buf[z * LO + q + 1]], axis=1)
             part = jnp.dot(r.hid_buf[...], pair, preferred_element_type=F32)
@@ -601,48 +614,46 @@
         if k > 0:
             spread(k - 1)
     spread(HI - 1)
-    CW = LO * W
+
+    def drain():
+        for z in range(1, HI):
+
+            @pl.when(hi + z < HI)
+            def _():
+                sent(r.kv_buf.at[0], r.k_send.at[z])
+                sent(r.bias_in.at[0], r.b_send.at[z])
+
+        sent(r.kv_buf.at[0, pl.ds(0, (LO - 1) * T)], r.k_send.at[0])
+        sent(r.bias_in.at[0, pl.ds(0, LO - 1)], r.b_send.at[0])
+        sent(r.q_in.at[pl.ds(0, LO - 1)], r.q_send.at[0])
+        sent(r.att_pl.at[pl.ds(0, (LO - 1) * T)], r.t_send.at[0])
+        sent(up.blocks(HI - 1), r.wz_send.at[0])
+        sent(dn.blocks(HI - 1), r.wz_send.at[1])
+        up.wait_sent(HI)
+        dn.wait_sent(HI)
+        for z in range(HI):
+
+            @pl.when((z <= hi) & (hi + 1 < HI))
+            def _():
+                sent(r.res_buf, r.nu_send.at[z])
+
+            @pl.when((z >= hi) & (hi > 0))
+            def _():
+                sent(r.res_buf, r.nd_send.at[z])
+
+        sent(r.n_buf.at[pl.ds(0, HI * H)], r.np_send.at[0])
+        sent(r.x_in, r.x_send.at[0])
+
+    scoped("drain", drain)
     for k in range(HI):
         z = nth(k)
         cols = pl.ds(pl.multiple_of(z * CW, LANES), CW)
         update = r.xs_buf[z, pl.ds(hi * H, H), :].astype(F32)
+        scoped(f"sum_wait{k}", arrived, r.pr_buf.at[z, pl.ds(0, HI - 1)], r.p_recv.at[z])
         for far in range(1, HI):
-            src = (hi + HI - far) % HI
-            arrived(r.pr_buf.at[src, z], r.p_recv.at[src * HI + z])
-            update = update + r.pr_buf[src, z].astype(F32)
+            update = update + r.pr_buf[z, (hi + far) % HI].astype(F32)
         r.out_ref[:, cols] = (r.res_buf[:, cols].astype(F32) + update).astype(BF16)
-
-    for k, p in enumerate(peers):
-        for copy in spread_heads(k, p):
-            copy.wait_send()
-        att_back(k, p).wait_send()
-    for z in range(HI):
-
-        @pl.when(z != hi)
-        def _():
-            up_far(z).wait_send()
-            dn_far(z).wait_send()
-
-        for copy in up.direct(z) + up.diag(z) + dn.direct(z) + dn.diag(z):
-            copy.wait_send()
-
-        @pl.when((z <= hi) & (hi + 1 < HI))
-        def _():
-            for copy in keys_up(z):
-                copy.wait_send()
-            for q in range(NC):
-                n_up(z, q).wait_send()
-
-        @pl.when((z >= hi) & (hi > 0))
-        def _():
-            for q in range(NC):
-                n_down(z, q).wait_send()
-
-        for q in range(NC):
-            n_pass(z, q).wait_send()
-        x_out(z).wait_send()
-        for far in range(1, HI):
-            p_out(z, far).wait_send()
+    sent(r.pr_buf.at[:, pl.ds(0, HI - 1)], r.p_send.at[0])
 
 
 def fits(tokens, queries, key_values, stop_bias, up_proj, down_proj):
@@ -651,8 +662,7 @@
     hidden = up_proj.shape[1]
     return (
         lax.axis_size("tp") == 2
-        and sp % LO == 0
-        and sp > LO
+        and sp == LO * LO
         and seqs == 1
         and heads == 2 * LO
         and queries.shape[2] == heads * HEAD
@@ -692,7 +702,7 @@
         tok_hbm=(tokens.reshape(T, D), hbm),
         q_hbm=(queries.reshape(T, queries.shape[2]), hbm),
         kv_hbm=(key_values.reshape(T, key_values.shape[2]), hbm),
-        bias_ref=(stop_bias.reshape(T, heads).T, vmem),
+        bias_hbm=(stop_bias.reshape(T, heads).T, hbm),
         wo_hbm=(out_proj, hbm),
         gain_hbm=(norm_gain.reshape(1, D), hbm),
         up_hbm=(up_proj, hbm),
@@ -700,6 +710,7 @@
     )
     scratch = dict(
         tok_v=pltpu.VMEM((T, D), BF16),
+        bias_v=pltpu.VMEM((heads, T), BF16),
         q_v=pltpu.VMEM((T, G * LANES), BF16),
         kv_v=pltpu.VMEM((T, G * LANES), BF16),
         wo_v=pltpu.VMEM(out_proj.shape, BF16),
@@ -708,9 +719,9 @@
         dn_v=pltpu.VMEM((hidden, W), BF16),
         up_buf=pltpu.VMEM((sp * R, CH), BF16),
         dn_buf=pltpu.VMEM((sp, CH, W), BF16),
-        bias_out=pltpu.VMEM((G, 2 * G, LANES), F32),
-        bias_in=pltpu.VMEM((LO, 2 * G, LANES), F32),
-        bias_pl=pltpu.VMEM((HI, 2 * G, PL), F32),
+        bias_out=pltpu.VMEM((G, 2, LANES), F32),
+        bias_in=pltpu.VMEM((HI, LO, 2, LANES), F32),
+        bias_pl=pltpu.VMEM((HI, 2, PL), F32),
         q_in=pltpu.VMEM((LO, T, LANES), BF16),
         q_all=pltpu.VMEM((2 * PL, LANES), BF16),
         kv_buf=pltpu.VMEM((HI, PL, LANES), BF16),
@@ -728,39 +739,41 @@
         x_in=pltpu.VMEM((HI, HI * H, LO * W), BF16),
         xs_buf=pltpu.VMEM((HI, HI * H, LO * W), BF16),
         pr_buf=pltpu.VMEM((HI, HI, H, LO * W), BF16),
-        load_sem=sem(9),
-        a_send=sem(9),
-        k_recv=sem(LO),
-        q_recv=sem(LO),
-        b_recv=sem(LO),
-        kz_send=sem(2 * HI),
-        kz_recv=sem(HI),
-        bz_recv=sem(HI),
-        wz_send=sem(HI * 2),
-        up_sp=sem(HI * 4),
-        up_recv=sem(sp),
-        up_half=sem(HI),
-        dn_sp=sem(HI * 4),
-        dn_recv=sem(sp),
-        dn_half=sem(HI),
-        t_send=sem(3),
-        t_recv=sem(LO),
+        load_sem=sem(10),
+        k_send=sem(HI),
+        b_send=sem(HI),
+        ready=pltpu.SemaphoreType.REGULAR,
+        q_send=sem(1),
+        k_recv=sem(HI),
+        b_recv=sem(HI),
+        q_recv=sem(1),
+        wz_send=sem(2),
+        up_sp=sem(1),
+        up_own=sem(HI),
+        up_near=sem(HI),
+        up_diag=sem(HI),
+        dn_sp=sem(1),
+        dn_own=sem(HI),
+        dn_near=sem(HI),
+        dn_diag=sem(HI),
+        t_send=sem(1),
+        t_recv=sem(1),
         pj_send=pltpu.SemaphoreType.DMA,
         pj_recv=pltpu.SemaphoreType.DMA,
-        nu_send=sem(HI * NC),
-        nd_send=sem(HI * NC),
-        np_send=sem(HI * NC),
+        nu_send=sem(HI),
+        nd_send=sem(HI),
+        np_send=sem(1),
         nz_recv=sem(HI * NC),
-        nc_recv=sem(HI * NC),
-        x_send=sem(HI),
+        nc_recv=sem(1),
+        x_send=sem(1),
         x_recv=sem(HI),
-        p_send=sem(HI * HI),
-        p_recv=sem(HI * HI),
+        p_send=sem(1),
+        p_recv=sem(HI),
     )
     names = [*operands, "out_ref", *scratch]
     out = pl.pallas_call(
         lambda *refs: layer_kernel(HI, G, NC, names, *refs),
-        out_shape=jax.ShapeDtypeStruct((H, D), BF16),
+        out_shape=pltpu.VMEM((H, D), BF16),
         in_specs=[spec for _, spec in operands.values()],
         out_specs=vmem,
         scratch_shapes=list(scratch.values()),

time: 78.7 us -> 60.9 us (0.77)
  Pallas kernels: 77 us -> 60 us
  local copies, waits for them, and re-layouts: 1.57 us -> 0.66 us
    pallas_call x1, Pallas kernels: 77 us -> 60 us  [body(): pl.pallas_call(lambda *refs: layer_kernel(HI, G, NC, names, *refs), out_s...]
    unnamed x1, local copies, waits for them, and re-layouts: 1.57 us -> 0.66 us
where the time goes in v2:
time: 60.9 us; the launch traced here: 60.7 us
  Pallas kernels  60 us (99%)
  local copies, waits for them, and re-layouts  0.66 us (1%)
    pallas_call x1, Pallas kernels, body(): pl.pallas_call(lambda *refs: layer_kernel(HI, G, NC, names, *refs), out_s...  60 us

profile of v2, /device:TPU:0, one launch (start us, length us, event | category | flops | bytes accessed | tf_op | source)
XLA Modules:
  0.0 60.7 jit_solution(18220997023258317242)
XLA Ops:
  0.0 60.0 %layer.1 = bf16[32,2048]{1,0:T(8,128)(2,1)S(1)} custom-call(bf16[64,2048]{1,0:T(8,128)(2,1)} %bitcast.9, bf16[64,512]{1,0:T(8,128)(2,1)} %bitcast.10, bf16[64,512]{1,0:T(8,128)(2,1)} %bitcast.11, bf16[8,64]{1,0:T(8,128)(2,1)} %bitcast.13, bf16[512,2048]{1,0:T(8,128)(2,1)} %refs_4_.1, f32[1,2048]{1,0:T(1,128)} %bitcast.12, bf16[128,2048]{1,0:T(8,128)(2,1)} %refs_6_.1, ...), custom_call_target="tpu_custom_call" | custom-call | tf_op jit(solution)/shard_map/layer/pallas_call | solution.py:774
  60.0 0.7 %copy.10 = bf16[32,1,2048]{2,0,1:T(8,128)(2,1)} copy(bf16[32,1,2048]{2,0,1:T(8,128)(2,1)S(1)} %bitcast.8) | data formatting | bytes 262144

commit v3 on v2

--- a/solution.py
+++ b/solution.py
@@ -364,6 +364,15 @@
         near = hi + (k + 1) // 2 if k % 2 else hi - k // 2
         return jnp.where(k <= 2 * small, near, hi + tilt * (k - small))
 
+    upper = hi // (HI // 2)
+    rank = hi + upper * (HI - 1 - 2 * hi)
+
+    def order(k):
+        if k == 0:
+            return hi
+        z = k - 1 + (rank < k).astype(jnp.int32)
+        return z + upper * (HI - 1 - 2 * z)
+
     def below(far, d):
         @pl.when(hi >= d)
         def _():
@@ -389,13 +398,18 @@
                     start(send_keys(d, p))
 
     raise_keys((lo,))
+    pair = hi + 1 - 2 * (hi % 2)
     for d in range(1, HI):
         below(up_far, d)
+        if d == 1:
+            pl.when(hi % 2 == 1)(lambda: dn_far(pair).start())
     scoped("ready", pl.semaphore_wait, r.ready, LO - 1)
     raise_keys(peers)
     start(up.direct(hi, r.up_v.at[:, own_cols]))
     for d in range(1, HI):
         above(up_far, d)
+        if d == 1:
+            pl.when(hi % 2 == 0)(lambda: dn_far(pair).start())
     start(dn.direct(hi, r.dn_v.at[pl.ds(hi * CH, CH)]))
 
     r.q_in[lo] = r.q_v[:, own_lanes]
@@ -459,12 +473,14 @@
             scoped(f"attend{d}", attend, z, False)
 
     def relay_direct(piece, k):
-        scoped(f"own_wait{k}", piece.wait_own, nth(k))
-        start(piece.direct(nth(k)))
+        z = nth(k) if piece is up else order(k)
+        scoped(f"{'UD'[piece is dn]}own_wait{k}", piece.wait_own, z)
+        start(piece.direct(z))
 
     def relay_diag(piece, k):
-        scoped(f"direct_wait{k}", piece.wait_direct, nth(k))
-        start(piece.diag(nth(k)))
+        z = nth(k) if piece is up else order(k)
+        scoped(f"{'UD'[piece is dn]}direct_wait{k}", piece.wait_direct, z)
+        start(piece.diag(z))
 
     scoped("attend0", attend, hi, True)
     relay_diag(up, 0)
@@ -483,11 +499,21 @@
 
     for p in peers:
         att_back(p).start()
-    for d in range(1, HI):
-        below(dn_far, d)
-        above(dn_far, d)
+
+    def dn_rest():
+        for d in range(1, HI):
+
+            @pl.when((hi >= d) & (hi - d != pair))
+            def _():
+                dn_far(hi - d).start()
+
+            @pl.when((hi + d < HI) & (hi + d != pair))
+            def _():
+                dn_far(hi + d).start()
+
+    r.att_buf[:, own_lanes] = r.att_pl[pl.ds(lo * T, T), :]
     relay_diag(dn, 0)
-    r.att_buf[:, own_lanes] = r.att_pl[pl.ds(lo * T, T), :]
+    pl.when(upper == 0)(lambda: relay_direct(up, 2))
     with jax.named_scope("att_wait"):
         for load in loads[5:]:
             load.wait()
@@ -500,8 +526,10 @@
         r.pj_buf[:, cols] = jnp.dot(att, r.wo_v[:, cols], preferred_element_type=F32).astype(BF16)
     pj_copy = remote(r.pj_buf.at[pl.ds(other * H, H)], r.pj_in, r.pj_send, r.pj_recv, s, other)
     pj_copy.start()
-    relay_direct(up, 2)
+    dn_rest()
     relay_diag(up, 1)
+    relay_direct(dn, 1)
+    pl.when(upper == 1)(lambda: relay_direct(up, 2))
     scoped("pj_wait", pj_copy.wait)
     mine = pl.ds(c * H, H)
     total = r.pj_buf[mine, :].astype(F32) + r.pj_in[...].astype(F32)
@@ -538,12 +566,8 @@
     for q in range(NC):
         n_pass(hi, q).start()
 
-    upper = hi // (HI // 2)
-
     def norm_take(k):
-        rank = hi + upper * (HI - 1 - 2 * hi)
-        z = k - 1 + (rank < k).astype(jnp.int32)
-        z = z + upper * (HI - 1 - 2 * z)
+        z = order(k)
         for q in range(NC):
             scoped(f"norm_wait{k}", arrived, n_at(z, c, q), r.nz_recv.at[z * NC + q])
 
@@ -557,18 +581,16 @@
 
             n_pass(z, q).start()
 
-    for k in range(3, HI):
-        relay_direct(up, k)
-        relay_diag(up, k - 1)
-    relay_direct(dn, 1)
-    for k in range(1, HI):
-        norm_take(k)
-        if k == 1:
-            relay_diag(up, HI - 1)
-        else:
-            relay_diag(dn, k - 1)
-        if k + 1 < HI:
-            relay_direct(dn, k + 1)
+    relay_direct(up, 3)
+    relay_diag(up, 2)
+    relay_diag(dn, 1)
+    norm_take(1)
+    relay_diag(up, 3)
+    relay_direct(dn, 2)
+    norm_take(2)
+    relay_direct(dn, 3)
+    norm_take(3)
+    relay_diag(dn, 2)
     with jax.named_scope("norm_other_wait"):
         arrived(r.n_buf.at[pl.ds(0, HI * H)], r.nc_recv.at[0])
     with jax.named_scope("up_wait"):
@@ -585,26 +607,30 @@
     mine_rows = pl.ds(c * half, half)
 
     def x_out(k):
-        z = nth(k)
+        z = order(k)
         rows = pl.ds(other * half, half)
         return remote(r.ps_buf.at[z, rows], r.x_in.at[z], r.x_send.at[0], r.x_recv.at[z], s, other)
 
-    def p_out(z, far):
-        hp = (hi + far) % HI
+    edge = (hi == 0) | (hi == HI - 1)
+    near = hi + 1 - 2 * (hi % 2)
+    away = (1 - upper) * (HI - 1)
+    middle = away + 2 * upper - 1
+
+    def p_out(z, hp):
         return remote(r.xs_buf.at[z, pl.ds(hp * H, H)], r.pr_buf.at[z, hi], r.p_send.at[0], r.p_recv.at[z], hp * LO + lo, c)
 
     def spread(k):
-        z = nth(k)
+        z = order(k)
         scoped(f"x_wait{k}", arrived, r.x_in.at[z], r.x_recv.at[z])
         mixed = r.ps_buf[z, mine_rows, :].astype(F32) + r.x_in[z].astype(F32)
         r.xs_buf[z] = mixed.astype(BF16)
 
-        for far in range(1, HI):
-            p_out(z, far).start()
-
-    relay_diag(dn, HI - 1)
+        p_out(z, away).start()
+        p_out(z, middle).start()
+        pl.when(jnp.logical_not(edge))(lambda: p_out(z, near).start())
+
     for k in range(HI):
-        z = nth(k)
+        z = order(k)
         scoped(f"dn_wait{k}", dn.wait_diag, z)
         for q in range(0, LO, 2):
             pair = jnp.concatenate([r.dn_buf[z * LO + q], r.dn_buf[z * LO + q + 1]], axis=1)
@@ -613,7 +639,14 @@
         x_out(k).start()
         if k > 0:
             spread(k - 1)
+        if k == 1:
+            relay_diag(dn, HI - 1)
     spread(HI - 1)
+
+    @pl.when(edge)
+    def _():
+        for k in range(HI):
+            p_out(order(k), near).start()
 
     def drain():
         for z in range(1, HI):
@@ -646,7 +679,7 @@
 
     scoped("drain", drain)
     for k in range(HI):
-        z = nth(k)
+        z = order(k)
         cols = pl.ds(pl.multiple_of(z * CW, LANES), CW)
         update = r.xs_buf[z, pl.ds(hi * H, H), :].astype(F32)
         scoped(f"sum_wait{k}", arrived, r.pr_buf.at[z, pl.ds(0, HI - 1)], r.p_recv.at[z])

time: 60.9 us -> 58.9 us (0.967)
  Pallas kernels: 60 us -> 58 us
    pallas_call x1, Pallas kernels: 60 us -> 58 us  [body(): pl.pallas_call(lambda *refs: layer_kernel(HI, G, NC, names, *refs), out_s...]
where the time goes in v3:
time: 58.9 us; the launch traced here: 58.7 us
  Pallas kernels  58 us (98%)
  local copies, waits for them, and re-layouts  0.66 us (1%)
    pallas_call x1, Pallas kernels, body(): pl.pallas_call(lambda *refs: layer_kernel(HI, G, NC, names, *refs), out_s...  58 us

profile of v3, /device:TPU:0, one launch (start us, length us, event | category | flops | bytes accessed | tf_op | source)
XLA Modules:
  0.0 58.7 jit_solution(15011658878614307060)
XLA Ops:
  0.0 58.0 %layer.1 = bf16[32,2048]{1,0:T(8,128)(2,1)S(1)} custom-call(bf16[64,2048]{1,0:T(8,128)(2,1)} %bitcast.9, bf16[64,512]{1,0:T(8,128)(2,1)} %bitcast.10, bf16[64,512]{1,0:T(8,128)(2,1)} %bitcast.11, bf16[8,64]{1,0:T(8,128)(2,1)} %bitcast.13, bf16[512,2048]{1,0:T(8,128)(2,1)} %refs_4_.1, f32[1,2048]{1,0:T(1,128)} %bitcast.12, bf16[128,2048]{1,0:T(8,128)(2,1)} %refs_6_.1, ...), custom_call_target="tpu_custom_call" | custom-call | tf_op jit(solution)/shard_map/layer/pallas_call | solution.py:807
  58.1 0.7 %copy.10 = bf16[32,1,2048]{2,0,1:T(8,128)(2,1)} copy(bf16[32,1,2048]{2,0,1:T(8,128)(2,1)S(1)} %bitcast.8) | data formatting | bytes 262144

commit v4 on v3

--- a/solution.py
+++ b/solution.py
@@ -292,7 +292,7 @@
         (r.gain_hbm, r.gain_v),
     ]
     loads = [pltpu.make_async_copy(a, b, r.load_sem.at[i]) for i, (a, b) in enumerate(local)]
-    start(loads)
+    start(loads[:5])
     loads[0].wait()
 
     half_lane = lax.broadcasted_iota(jnp.int32, (2 * G, LANES), 1) // HEAD
@@ -301,7 +301,7 @@
     for g in range(G):
         r.bias_out[g] = bias[2 * g : 2 * g + 2]
     with jax.named_scope("barrier"):
-        for load in loads[1:5]:
+        for load in loads[1:3]:
             load.wait()
         pl.semaphore_wait(barrier, 4 + (HI - 1))
 
@@ -398,6 +398,9 @@
                     start(send_keys(d, p))
 
     raise_keys((lo,))
+    start(loads[5:])
+    for load in loads[3:5]:
+        load.wait()
     pair = hi + 1 - 2 * (hi % 2)
     for d in range(1, HI):
         below(up_far, d)
@@ -500,17 +503,22 @@
     for p in peers:
         att_back(p).start()
 
-    def dn_rest():
+    def dn_below():
         for d in range(1, HI):
 
             @pl.when((hi >= d) & (hi - d != pair))
             def _():
                 dn_far(hi - d).start()
 
+    def dn_above():
+        for d in range(1, HI):
+
             @pl.when((hi + d < HI) & (hi + d != pair))
             def _():
                 dn_far(hi + d).start()
 
+    dn_below()
+    pl.when(hi == 0)(dn_above)
     r.att_buf[:, own_lanes] = r.att_pl[pl.ds(lo * T, T), :]
     relay_diag(dn, 0)
     pl.when(upper == 0)(lambda: relay_direct(up, 2))
@@ -526,7 +534,7 @@
         r.pj_buf[:, cols] = jnp.dot(att, r.wo_v[:, cols], preferred_element_type=F32).astype(BF16)
     pj_copy = remote(r.pj_buf.at[pl.ds(other * H, H)], r.pj_in, r.pj_send, r.pj_recv, s, other)
     pj_copy.start()
-    dn_rest()
+    pl.when(hi > 0)(dn_above)
     relay_diag(up, 1)
     relay_direct(dn, 1)
     pl.when(upper == 1)(lambda: relay_direct(up, 2))

time: 58.9 us -> 58.3 us (0.990)
    pallas_call x1, Pallas kernels: 58 us -> 57.5 us  [body(): pl.pallas_call(lambda *refs: layer_kernel(HI, G, NC, names, *refs), out_s...]
where the time goes in v4:
time: 58.3 us; the launch traced here: 58.1 us
  Pallas kernels  57.5 us (99%)
  local copies, waits for them, and re-layouts  0.66 us (1%)
    pallas_call x1, Pallas kernels, body(): pl.pallas_call(lambda *refs: layer_kernel(HI, G, NC, names, *refs), out_s...  57.5 us

profile of v4, /device:TPU:0, one launch (start us, length us, event | category | flops | bytes accessed | tf_op | source)
XLA Modules:
  0.0 58.1 jit_solution(11233656987792147098)
XLA Ops:
  0.0 57.5 %layer.1 = bf16[32,2048]{1,0:T(8,128)(2,1)S(1)} custom-call(bf16[64,2048]{1,0:T(8,128)(2,1)} %bitcast.9, bf16[64,512]{1,0:T(8,128)(2,1)} %bitcast.10, bf16[64,512]{1,0:T(8,128)(2,1)} %bitcast.11, bf16[8,64]{1,0:T(8,128)(2,1)} %bitcast.13, bf16[512,2048]{1,0:T(8,128)(2,1)} %refs_4_.1, f32[1,2048]{1,0:T(1,128)} %bitcast.12, bf16[128,2048]{1,0:T(8,128)(2,1)} %refs_6_.1, ...), custom_call_target="tpu_custom_call" | custom-call | tf_op jit(solution)/shard_map/layer/pallas_call | solution.py:815
  57.5 0.7 %copy.10 = bf16[32,1,2048]{2,0,1:T(8,128)(2,1)} copy(bf16[32,1,2048]{2,0,1:T(8,128)(2,1)S(1)} %bitcast.8) | data formatting | bytes 262144

commit v5 on v4

--- a/solution.py
+++ b/solution.py
@@ -599,18 +599,24 @@
     relay_direct(dn, 3)
     norm_take(3)
     relay_diag(dn, 2)
-    with jax.named_scope("norm_other_wait"):
-        arrived(r.n_buf.at[pl.ds(0, HI * H)], r.nc_recv.at[0])
+    half = HI * H
+    wide = 256 if CH % 256 == 0 else LANES
+
+    def hide(core):
+        rows = pl.ds(pl.multiple_of(core * half, half), half)
+        for i in range(CH // wide):
+            cols = slice(i * wide, (i + 1) * wide)
+            raw = jnp.maximum(jnp.dot(r.n_buf[rows, :], r.up_buf[:, cols], preferred_element_type=F32), 0.0)
+            r.hid_buf[rows, cols] = (raw * raw).astype(BF16)
+
     with jax.named_scope("up_wait"):
         for k in range(HI):
             up.wait_diag(nth(k))
-
-    wide = 256 if CH % 256 == 0 else LANES
-    for i in range(CH // wide):
-        cols = slice(i * wide, (i + 1) * wide)
-        raw = jnp.maximum(jnp.dot(r.n_buf[...], r.up_buf[:, cols], preferred_element_type=F32), 0.0)
-        r.hid_buf[:, cols] = (raw * raw).astype(BF16)
-    half = HI * H
+    hide(c)
+    with jax.named_scope("norm_other_wait"):
+        arrived(r.n_buf.at[pl.ds(0, HI * H)], r.nc_recv.at[0])
+    hide(other)
+
     CW = LO * W
     mine_rows = pl.ds(c * half, half)
 

time: 58.3 us -> 58.7 us (level)
  no operation moved by 1% of the time
where the time goes in v5:
time: 58.7 us; the launch traced here: 58.6 us
  Pallas kernels  57.9 us (99%)
  local copies, waits for them, and re-layouts  0.66 us (1%)
    pallas_call x1, Pallas kernels, body(): pl.pallas_call(lambda *refs: layer_kernel(HI, G, NC, names, *refs), out_s...  57.9 us

profile of v5, /device:TPU:0, one launch (start us, length us, event | category | flops | bytes accessed | tf_op | source)
XLA Modules:
  0.0 58.6 jit_solution(14904505016707220810)
XLA Ops:
  0.0 57.9 %layer.1 = bf16[32,2048]{1,0:T(8,128)(2,1)S(1)} custom-call(bf16[64,2048]{1,0:T(8,128)(2,1)} %bitcast.9, bf16[64,512]{1,0:T(8,128)(2,1)} %bitcast.10, bf16[64,512]{1,0:T(8,128)(2,1)} %bitcast.11, bf16[8,64]{1,0:T(8,128)(2,1)} %bitcast.13, bf16[512,2048]{1,0:T(8,128)(2,1)} %refs_4_.1, f32[1,2048]{1,0:T(1,128)} %bitcast.12, bf16[128,2048]{1,0:T(8,128)(2,1)} %refs_6_.1, ...), custom_call_target="tpu_custom_call" | custom-call | tf_op jit(solution)/shard_map/layer/pallas_call | solution.py:821
  57.9 0.7 %copy.10 = bf16[32,1,2048]{2,0,1:T(8,128)(2,1)} copy(bf16[32,1,2048]{2,0,1:T(8,128)(2,1)S(1)} %bitcast.8) | data formatting | bytes 262144
